TPU v7x, 256 devices: a 4x2x16 block of a 4x16x16 slice. The times are simulated.
256 devices in a mesh: grp: 2 (over y), kv: 32 (over z, core), tp: 4 (over x).
Axes of the slice: x: 4, y: 2, z: 16, core: 2. Of those that a mesh axis runs over, the one named last changes fastest.
The devices are a block of a 4x16x16 slice.
Arguments:
- tokens: bfloat16 [16, 16, 4096], P('grp'), parts along dimension 0, may hold values from -6 to 6
- norm_gain: bfloat16 [4096], replicated, may hold values from 0.099609375 to 1.8984375
- query_weight: bfloat16 [4096, 4096], P('kv', 'tp'), may hold values from -0.09375 to 0.09375
- key_weight: bfloat16 [4096, 1024], P('kv', 'tp'), may hold values from -0.15625 to 0.15625
- value_weight: bfloat16 [4096, 1024], P('kv', 'tp'), may hold values from -0.09375 to 0.09375
- out_weight: bfloat16 [4096, 4096], P(None, 'kv'), may hold values from -0.09375 to 0.09375
- head_gain: bfloat16 [128], replicated, may hold values from 0.099609375 to 1.8984375
- mix_lambda: float32 [32], P('tp'), may hold values from 0.3 to 0.8
- cache_keys: bfloat16 [16, 8, 16384, 128], P('grp', 'tp', 'kv'), parts along dimension 0, may hold values from -310 to 310
- cache_values: bfloat16 [16, 8, 16384, 128], P('grp', 'tp', 'kv'), parts along dimension 0, may hold values from -6 to 6
- lengths: int32 [16], P('grp'), parts along dimension 0, may hold values from 8192 to 16360, as said below
- accepted: int32 [16], P('grp'), parts along dimension 0, may hold values from 0 to 8
- parents: int32 [16, 16], P('grp'), parts along dimension 0, may hold values from 0 to 15, as said below
Outputs:
- mixed: bfloat16 [16, 16, 4096], P('grp', None, 'kv'), parts along dimension 0
- keys_out: bfloat16 [16, 8, 16384, 128], P('grp', 'tp', 'kv'), parts along dimension 0
- values_out: bfloat16 [16, 8, 16384, 128], P('grp', 'tp', 'kv'), parts along dimension 0
There are 2 independent parts, one for each index of `grp`. A program takes and returns all parts, laid end to end along the dimension named above; an argument that names none is the same for every part. Nothing has to cross between parts.
Inputs may be any that keep to these rules, and one draw needn't show every extreme that they name: `lengths`: one sequence has exactly the largest length in every draw. `parents`: proposal 0 is the root and names itself; every other proposal i names one of 0 to i - 1.
All inputs are finite; a program needn't handle non-finite values.
Results may differ from a plain program's by a relative error of at most 0.014.
The roundings to bfloat16 on the way count: a program that leaves them out, or rounds other values in their place, can miss the bound.
Values may be sent and summed in bfloat16 or wider, within the bound.
No kernel may reach another device: no remote copies, remote signals or barrier semaphores. Data moves between devices by JAX's collectives and lax.ppermute only.
A program may use at most 128 MiB of HBM per device.

v0:
```python
import jax
import jax.numpy as jnp
from jax import lax
from jax.sharding import PartitionSpec as P

NEG_FILL = -1e30
ROTARY_BASE = 10000.0
NORM_EPS = 1e-06


def in_blocks(x, dim, peers):
    before, after = (x.shape[:dim], x.shape[dim + 1 :])
    return jnp.moveaxis(x.reshape(*before, peers, -1, *after), dim, 0)


def sum_at_owner(x, axis, dim):
    peers = lax.axis_size(axis)
    tiles = lax.all_to_all(in_blocks(x, dim, peers), axis, 0, 0, tiled=True)
    return jnp.sum(tiles, axis=0)


def copy_for_each(x, axis):
    copies = jnp.broadcast_to(x, (lax.axis_size(axis), *x.shape))
    return lax.all_to_all(copies, axis, split_axis=0, concat_axis=0, tiled=True)


def in_order(tiles, dim):
    dims = list(tiles.shape[1:])
    dims[dim] *= tiles.shape[0]
    return jnp.moveaxis(tiles, 0, dim).reshape(dims)


def gathered_copies(x, axis, dim):
    tiles = copy_for_each(x, axis)
    return in_order(tiles, dim)


def taken_together(x, axis):
    return copy_for_each(x, axis).astype(jnp.float32).sum(axis=0)


def ancestry(parents):
    proposals = parents.shape[-1]
    indices = jnp.arange(proposals, dtype=jnp.int32)
    linked = (parents[:, :, None] == indices[None, None, :]) & (indices[None, :, None] > 0)
    reach = jnp.minimum(
        linked.astype(jnp.float32) + jnp.eye(proposals, dtype=jnp.float32)[None], 1.0
    )
    for squaring in range(proposals.bit_length()):
        reach = jnp.minimum(jnp.einsum("bij,bjk->bik", reach, reach), 1.0)
    return reach


def rotate(vectors, positions):
    half_dim = vectors.shape[-1] // 2
    inverse = ROTARY_BASE ** (-jnp.arange(half_dim, dtype=jnp.float32) / half_dim)
    angles = positions.astype(jnp.float32)[..., None, None] * inverse
    cosine = jnp.cos(angles)
    sine_part = jnp.sin(angles)
    first_half = vectors[..., :half_dim]
    second_half = vectors[..., half_dim:]
    return jnp.concatenate(
        [
            first_half * cosine - second_half * sine_part,
            second_half * cosine + first_half * sine_part,
        ],
        axis=-1,
    )


def block_partials(query_maps, block_keys, block_values, allowed):
    qk_dim = query_maps.shape[-1]
    highs, totals, sums = ([], [], [])
    for which in range(2):
        key_map = block_keys[..., which * qk_dim : (which + 1) * qk_dim]
        scores = jnp.einsum(
            "bgrpd,bgsd->bgrps", query_maps[which], key_map, preferred_element_type=jnp.float32
        ) * qk_dim ** (-0.5)
        scores = jnp.where(allowed[:, None, None], scores, NEG_FILL)
        highest = jnp.max(scores, axis=-1)
        weights = jnp.where(allowed[:, None, None], jnp.exp(scores - highest[..., None]), 0.0)
        highs.append(highest)
        totals.append(jnp.sum(weights, axis=-1))
        sums.append(
            jnp.einsum(
                "bgrps,bgsv->bgrpv",
                weights.astype(jnp.bfloat16),
                block_values,
                preferred_element_type=jnp.float32,
            ).astype(jnp.bfloat16)
        )
    return (jnp.stack(highs), jnp.stack(totals), jnp.stack(sums))


def absorb(carry, pieces):
    highest, total_sum, acc_sum = carry
    piece_high, piece_total, piece_acc = pieces
    new_high = jnp.maximum(highest, jnp.max(piece_high, axis=0))
    scaling = jnp.exp(piece_high - new_high[None])
    new_total = jnp.sum(piece_total * scaling, axis=0)
    new_acc = jnp.sum(piece_acc.astype(jnp.float32) * scaling[..., None], axis=0)
    return (new_high, new_total, new_acc)


def on_device(
    tokens,
    norm_gain,
    query_weight,
    key_weight,
    value_weight,
    out_weight,
    head_gain,
    mix_lambda,
    cache_keys,
    cache_values,
    lengths,
    accepted,
    parents,
):
    seqs, proposals, width = tokens.shape
    shard_index = lax.axis_index("kv")
    slab = query_weight.shape[0]
    local_heads = mix_lambda.shape[0]
    local_kv = cache_keys.shape[1]
    group = local_heads // local_kv
    span_len = cache_keys.shape[2]
    qk_dim = cache_keys.shape[-1] // 2
    v_dim = cache_values.shape[-1]
    query_cols = query_weight.shape[1]
    key_cols = key_weight.shape[1]
    floats = tokens.astype(jnp.float32)
    normed = (
        floats
        * lax.rsqrt(jnp.mean(floats * floats, axis=-1, keepdims=True) + NORM_EPS)
        * norm_gain.astype(jnp.float32)
    ).astype(jnp.bfloat16)
    my_slab = lax.dynamic_slice_in_dim(normed, shard_index * slab, slab, 2).reshape(
        seqs * proposals, slab
    )
    partial_value = jnp.concatenate(
        [
            jnp.dot(my_slab, query_weight, preferred_element_type=jnp.float32),
            jnp.dot(my_slab, key_weight, preferred_element_type=jnp.float32),
            jnp.dot(my_slab, value_weight, preferred_element_type=jnp.float32),
        ],
        axis=1,
    )
    reach = ancestry(parents)
    depth = (jnp.sum(reach, axis=-1) - 1.0).astype(jnp.int32)
    starts = lengths + accepted
    position = (starts[:, None] + depth).reshape(seqs * proposals)
    my_rows = sum_at_owner(partial_value, "kv", 0)
    share = my_rows.shape[0]
    row_positions = lax.dynamic_slice_in_dim(position, shard_index * share, share, 0)
    turned_queries = rotate(
        my_rows[:, :query_cols].reshape(-1, query_cols // qk_dim, qk_dim), row_positions
    )
    turned_keys = rotate(
        my_rows[:, query_cols : query_cols + key_cols].reshape(-1, key_cols // qk_dim, qk_dim),
        row_positions,
    )
    projected = gathered_copies(
        jnp.concatenate(
            [
                turned_queries.reshape(-1, query_cols),
                turned_keys.reshape(-1, key_cols),
                my_rows[:, query_cols + key_cols :],
            ],
            axis=1,
        ).astype(jnp.bfloat16),
        "kv",
        0,
    )
    queries = projected[:, :query_cols].reshape(seqs, proposals, local_kv, group, 2, qk_dim)
    query_maps = jnp.transpose(queries, (4, 0, 2, 3, 1, 5))
    fresh_keys = jnp.transpose(
        projected[:, query_cols : query_cols + key_cols].reshape(
            seqs, proposals, local_kv, 2 * qk_dim
        ),
        (0, 2, 1, 3),
    )
    fresh_values = jnp.transpose(
        projected[:, query_cols + key_cols :].reshape(seqs, proposals, local_kv, v_dim),
        (0, 2, 1, 3),
    )
    offset = shard_index * span_len
    positions = offset + jnp.arange(span_len, dtype=jnp.int32)
    relative = positions[None, :] - starts[:, None]
    slots = (relative[:, :, None] == jnp.arange(proposals, dtype=jnp.int32)[None, None, :]).astype(
        jnp.float32
    )
    in_tree = jnp.einsum("bij,bsj->bis", reach, slots) > 0.5
    allowed = (relative < 0)[:, None, :] | in_tree
    written = ((relative >= 0) & (relative < proposals))[:, None, :, None]
    slot_table = slots.astype(jnp.bfloat16)
    placed_keys = jnp.einsum(
        "bsj,bgjc->bgsc", slot_table, fresh_keys, preferred_element_type=jnp.float32
    ).astype(jnp.bfloat16)
    placed_values = jnp.einsum(
        "bsj,bgjc->bgsc", slot_table, fresh_values, preferred_element_type=jnp.float32
    ).astype(jnp.bfloat16)
    keys_out = jnp.where(written, placed_keys, cache_keys)
    values_out = jnp.where(written, placed_values, cache_values)
    highs, totals, sums = block_partials(query_maps, keys_out, values_out, allowed)
    stat_shape = highs.shape
    initial = (
        jnp.full(stat_shape, NEG_FILL, jnp.float32),
        jnp.zeros(stat_shape, jnp.float32),
        jnp.zeros(stat_shape + (v_dim,), jnp.float32),
    )
    final = absorb(
        initial,
        (
            lax.all_gather(highs[None], "kv", axis=0, tiled=True),
            lax.all_gather(totals[None], "kv", axis=0, tiled=True),
            lax.all_gather(sums[None].astype(jnp.float32), "kv", axis=0, tiled=True).astype(
                jnp.bfloat16
            ),
        ),
    )
    attended = final[2] / final[1][..., None]
    lam_heads = mix_lambda.reshape(local_kv, group)[None, :, :, None, None]
    difference = attended[0] - lam_heads * attended[1]
    head_out = (
        difference
        * lax.rsqrt(jnp.mean(difference * difference, axis=-1, keepdims=True) + NORM_EPS)
        * head_gain.astype(jnp.float32)
    ).astype(jnp.bfloat16)
    head_rows = jnp.transpose(head_out, (0, 3, 1, 2, 4)).reshape(
        seqs, proposals, local_heads * v_dim
    )
    first_row = lax.axis_index("tp") * local_heads * v_dim
    my_weight = lax.dynamic_slice_in_dim(out_weight, first_row, local_heads * v_dim, 0)
    term = jnp.dot(
        head_rows.reshape(seqs * proposals, local_heads * v_dim),
        my_weight,
        preferred_element_type=jnp.float32,
    )
    mixed = taken_together(term.astype(jnp.bfloat16), "tp").astype(jnp.float32).astype(jnp.bfloat16)
    return (mixed.reshape(seqs, proposals, -1), keys_out, values_out)


def solution(mesh):
    in_specs = (
        P("grp", None, None),
        P(),
        P("kv", "tp"),
        P("kv", "tp"),
        P("kv", "tp"),
        P(None, "kv"),
        P(),
        P("tp"),
        P("grp", "tp", "kv", None),
        P("grp", "tp", "kv", None),
        P("grp"),
        P("grp"),
        P("grp", None),
    )
    out_specs = (P("grp", None, "kv"), P("grp", "tp", "kv", None), P("grp", "tp", "kv", None))
    return jax.shard_map(
        on_device, mesh=mesh, in_specs=in_specs, out_specs=out_specs, check_vma=False
    )
```

profile of v0, /device:TPU:33, one launch (start us, length us, event | category | flops | bytes accessed | tf_op | source)
XLA Modules:
  0.0 281.9 jit_solution(15675201665332809082)
XLA Ops:
  7.2 1.6 convert_element_type.89
  11.7 25.5 %all-to-all-start = ((f32[32,4,1536]{2,1,0:T(4,128)}), f32[32,4,1536]{2,1,0:T(4,128)S(1)}, u32[]{:S(2)}, u32[]{:S(2)}) async-start(f32[32,4,1536]{2,1,0:T(4,128)} %reshape.263), calls=%async_computation | async-start | bytes 1572864 | tf_op jit(solution)/shard_map/all_to_all | solution.py:18
  39.1 42.5 %all-to-all-done = f32[32,4,1536]{2,1,0:T(4,128)S(1)} async-done(((f32[32,4,1536]{2,1,0:T(4,128)}), f32[32,4,1536]{2,1,0:T(4,128)S(1)}, u32[]{:S(2)}, u32[]{:S(2)}) %all-to-all-start) | async-done | bytes 786464 | tf_op jit(solution)/shard_map/all_to_all | solution.py:18
  83.3 4.3 %all-to-all-start.1 = ((bf16[32,4,1536]{2,1,0:T(4,128)(2,1)}), bf16[32,4,1536]{2,1,0:T(4,128)(2,1)S(1)}, u32[]{:S(2)}, u32[]{:S(2)}) async-start(bf16[32,4,1536]{2,1,0:T(4,128)(2,1)} %broadcast_in_dim.82), calls=%async_computation.1 | async-start | bytes 786432 | tf_op jit(solution)/shard_map/all_to_all | solution.py:24
  87.7 3.9 %copy.107 = bf16[8,2,512,128]{2,3,1,0:T(8,128)(2,1)} copy(bf16[8,2,512,128]{3,2,1,0:T(8,128)(2,1)} %param.21) | data formatting | bytes 4194304 | tf_op args[8]
  91.6 2.9 %copy.109 = bf16[8,2,512,128]{2,3,1,0:T(8,128)(2,1)S(1)} copy(bf16[8,2,512,128]{3,2,1,0:T(8,128)(2,1)} %param.22) | data formatting | bytes 4194304 | tf_op args[9]
  95.8 1.6 fusion.22
  97.4 18.1 %all-to-all-done.1 = bf16[32,4,1536]{2,1,0:T(4,128)(2,1)S(1)} async-done(((bf16[32,4,1536]{2,1,0:T(4,128)(2,1)}), bf16[32,4,1536]{2,1,0:T(4,128)(2,1)S(1)}, u32[]{:S(2)}, u32[]{:S(2)}) %all-to-all-start.1) | async-done | bytes 393248 | tf_op jit(solution)/shard_map/all_to_all | solution.py:24
  116.3 1.5 fusion.76
  120.8 2.0 copy.143
  122.8 2.4 bitcast_select_fusion.1
  125.7 1.2 fusion.6
  131.0 2.3 fusion.8
  133.3 44.8 %all-gather.1 = f32[64,8,2,4,16]{4,1,3,2,0:T(8,128)S(1)} all-gather(f32[2,8,2,4,16]{4,1,3,2,0:T(8,128)S(1)} %copy.116), channel_id=3, replica_groups=mesh['grp'=2,'kv'=32,'tp'=4] {'kv'}, dimensions={0}, use_global_device_ids=true | all-gather | bytes 270336 | tf_op jit(solution)/shard_map/all_gather | solution.py:215
  178.1 2.1 copy.117
  180.3 48.5 %all-gather = f32[64,8,2,4,16]{4,1,3,2,0:T(8,128)S(1)} all-gather(f32[2,8,2,4,16]{4,1,3,2,0:T(8,128)S(1)} %copy.112), channel_id=2, replica_groups=mesh['grp'=2,'kv'=32,'tp'=4] {'kv'}, dimensions={0}, use_global_device_ids=true | all-gather | bytes 270336 | tf_op jit(solution)/shard_map/all_gather | solution.py:214
  228.7 2.1 copy.114
  231.2 3.0 %multiply_reduce_fusion.2 = (f32[2,8,2,4,16]{4,3,2,1,0:T(4,128)S(1)}, f32[32,2,8,2,4,16]{0,5,4,3,2,1:T(8,128)}) fusion(f32[32,2,8,2,4,16]{0,5,4,3,2,1:T(8,128)} %copy.117, f32[32,2,8,2,4,16]{0,5,4,3,2,1:T(8,128)} %copy.114, f32[2,8,2,4,16]{4,3,2,1,0:T(4,128)S(1)} %copy.113), kind=kLoop, calls=%fused_computation.34 | loop fusion | flops 194560 | bytes 802816 | tf_op jit(solution)/shard_map/reduce_sum | solution.py:100
  234.1 3.4 %copy.115 = f32[32,2,8,2,4,16]{5,4,3,2,1,0:T(4,128)S(1)} copy(f32[32,2,8,2,4,16]{0,5,4,3,2,1:T(8,128)} %get-tuple-element.27) | data formatting | bytes 524288 | tf_op jit(solution)/shard_map/exp | solution.py:99
  237.5 11.1 %all-gather.4.cloned.1.call-done = bf16[32,2,8,2,4,16,128]{6,5,4,3,2,1,0:T(8,128)(2,1)} async-done(((bf16[1,2,8,2,4,16,128]{6,5,4,3,2,1,0:T(8,128)(2,1)}), bf16[32,2,8,2,4,16,128]{6,5,4,3,2,1,0:T(8,128)(2,1)}) %all-gather.4.cloned.1.call-update) | async-done | bytes 16777232 | tf_op jit(solution)/shard_map/all_gather | solution.py:216
  248.5 11.5 %multiply_reduce_fusion = f32[2,8,2,4,16,128]{5,4,3,2,1,0:T(8,128)S(1)} fusion(f32[32,2,8,2,4,16]{5,4,3,2,1,0:T(4,128)S(1)} %copy.115, bf16[32,2,8,2,4,16,128]{6,5,4,3,2,1,0:T(8,128)(2,1)} %all-gather.4.cloned.1.call-done), kind=kLoop, calls=%fused_computation | loop fusion | flops 24903680 | bytes 18087936 | tf_op jit(solution)/shard_map/reduce_sum | solution.py:101
  263.8 4.3 %all-to-all-start.2 = ((bf16[4,128,128]{2,1,0:T(8,128)(2,1)}), bf16[4,128,128]{2,1,0:T(8,128)(2,1)S(1)}, u32[]{:S(2)}, u32[]{:S(2)}) async-start(bf16[4,128,128]{2,1,0:T(8,128)(2,1)} %broadcast_in_dim.89), calls=%async_computation.2 | async-start | bytes 262144 | tf_op jit(solution)/shard_map/all_to_all | solution.py:24
  268.1 2.4 copy.120
  270.5 3.9 %copy.121 = bf16[8,2,512,128]{3,2,1,0:T(8,128)(2,1)} copy(bf16[8,2,512,128]{2,3,1,0:T(8,128)(2,1)} %copy-done.3) | data formatting | bytes 4194304
  (104 shorter events, 20.7 us)
Async XLA Ops:
  7.2 255.7 %copy-start = (bf16[4096,128]{1,0:T(8,128)(2,1)S(1)}, bf16[4096,128]{1,0:T(8,128)(2,1)}, u32[]{:S(2)}) copy-start(bf16[4096,128]{1,0:T(8,128)(2,1)} %param.18) | copy-start | bytes 3145732
  7.2 1.6 copy-start.4
  7.2 2.8 copy-start.8
  7.2 2.9 %copy-start.9 = (bf16[128,256]{1,0:T(8,128)(2,1)S(1)}, bf16[128,256]{1,0:T(8,128)(2,1)}, u32[]{:S(2)}) copy-start(bf16[128,256]{1,0:T(8,128)(2,1)} %param.16) | copy-start | bytes 196612
  7.2 3.1 %copy-start.7 = (bf16[128,1024]{1,0:T(8,128)(2,1)S(1)}, bf16[128,1024]{1,0:T(8,128)(2,1)}, u32[]{:S(2)}) copy-start(bf16[128,1024]{1,0:T(8,128)(2,1)} %param.15) | copy-start | bytes 786436
  10.5 26.7 %copy-start.14 = (s32[8]{0:T(128)S(1)}, s32[8]{0:T(128)}, u32[]{:S(2)}) copy-start(s32[8]{0:T(128)} %param.23) | copy-start | bytes 100
  10.5 26.7 %copy-start.15 = (s32[8]{0:T(128)S(1)}, s32[8]{0:T(128)}, u32[]{:S(2)}) copy-start(s32[8]{0:T(128)} %param.24) | copy-start | bytes 100
  10.5 26.7 %copy-start.13 = (s32[8,16]{1,0:T(8,128)S(1)}, s32[8,16]{1,0:T(8,128)}, u32[]{:S(2)}) copy-start(s32[8,16]{1,0:T(8,128)} %param.25) | copy-start | bytes 1540
  11.7 69.9 %all-to-all-start = ((f32[32,4,1536]{2,1,0:T(4,128)}), f32[32,4,1536]{2,1,0:T(4,128)S(1)}, u32[]{:S(2)}, u32[]{:S(2)}) async-start(f32[32,4,1536]{2,1,0:T(4,128)} %reshape.263), calls=%async_computation | async-start | bytes 1572864 | tf_op jit(solution)/shard_map/all_to_all | solution.py:18
  37.2 57.2 %copy-start.12 = (s32[8]{0:T(128)}, s32[8]{0:T(128)S(1)}, u32[]{:S(2)}) copy-start(s32[8]{0:T(128)S(1)} %add.75) | copy-start | bytes 100
  83.3 32.1 %all-to-all-start.1 = ((bf16[32,4,1536]{2,1,0:T(4,128)(2,1)}), bf16[32,4,1536]{2,1,0:T(4,128)(2,1)S(1)}, u32[]{:S(2)}, u32[]{:S(2)}) async-start(bf16[32,4,1536]{2,1,0:T(4,128)(2,1)} %broadcast_in_dim.82), calls=%async_computation.1 | async-start | bytes 786432 | tf_op jit(solution)/shard_map/all_to_all | solution.py:24
  87.6 160.9 %all-gather.4.cloned.1.call-start = ((), (), s32[]{:S(2)}) async-start(), calls=%async_computation.3 | async-start | bytes 17301504 | tf_op jit(solution)/shard_map/all_gather | solution.py:216
  122.7 2.4 copy-start.6
  122.8 2.4 copy-start.10
  125.2 1.7 copy-start.1
  125.7 1.2 copy-start.11
  126.9 1.7 copy-start.5
  127.7 1.3 copy-start.3
  129.0 1.8 copy-start.16
  129.0 1.8 copy-start.17
  260.4 7.7 %copy-start.2 = (bf16[8,2,512,128]{2,3,1,0:T(8,128)(2,1)S(1)}, bf16[8,2,512,128]{2,3,1,0:T(8,128)(2,1)}, u32[]{:S(2)}) copy-start(bf16[8,2,512,128]{2,3,1,0:T(8,128)(2,1)} %copy-done.1) | copy-start | bytes 6291460
  263.8 10.6 %all-to-all-start.2 = ((bf16[4,128,128]{2,1,0:T(8,128)(2,1)}), bf16[4,128,128]{2,1,0:T(8,128)(2,1)S(1)}, u32[]{:S(2)}, u32[]{:S(2)}) async-start(bf16[4,128,128]{2,1,0:T(8,128)(2,1)} %broadcast_in_dim.89), calls=%async_computation.2 | async-start | bytes 262144 | tf_op jit(solution)/shard_map/all_to_all | solution.py:24
Sparse Core Ops, SparseCore 0:
  131.0 117.5 all-gather.3
where the time goes:
time: 283 us; the launch traced here: 282 us
  blocking collectives  93.3 us (33%)
  waiting for transfers between devices  71.7 us (25%)
  local copies, waits for them, and re-layouts  34.4 us (12%)
  starting transfers between devices  34.1 us (12%)
  other arithmetic  23.5 us (8%)
  between operations  14.6 us (5%)
  matrix products  10.3 us (4%)
    all_gather x1, blocking collectives, on_device(): lax.all_gather(highs[None], 'kv', axis=0, tiled=True)  48.5 us
    all_gather x1, blocking collectives, on_device(): lax.all_gather(totals[None], 'kv', axis=0, tiled=True)  44.8 us
    all_to_all x1, waiting for transfers between devices, sum_at_owner(): tiles = lax.all_to_all(in_blocks(x, dim, peers), axis, 0, 0, tiled=True)  42.5 us
    all_to_all x1, starting transfers between devices, sum_at_owner(): tiles = lax.all_to_all(in_blocks(x, dim, peers), axis, 0, 0, tiled=True)  25.5 us
    all_to_all x2, waiting for transfers between devices, copy_for_each(): return lax.all_to_all(copies, axis, split_axis=0, concat_axis=0, tiled=True)  18.1 us
    unnamed x40, local copies, waits for them, and re-layouts  13.6 us
    reduce_sum x1, other arithmetic, absorb(): jnp.sum(piece_acc.astype(jnp.float32) * scaling[..., None], axis=0)  11.5 us
    all_gather x1, waiting for transfers between devices, on_device(): lax.all_gather(sums[None].astype(jnp.float32), 'kv', axis=0, tiled=True)  11.1 us
  transfers between devices with their start and end apart: 4, of which 3 were waited for; matrix products, arithmetic and copies ran while one was open for 11% of the time, Pallas kernels for 0%

commit v1 on v0

v1 whole, which is shorter than its diff:
```python
import functools

import jax
import jax.numpy as jnp
from jax import lax
from jax.experimental import pallas as pl
from jax.experimental.pallas import tpu as pltpu
from jax.sharding import PartitionSpec as P

NEG_FILL = -1e30
ROTARY_BASE = 10000.0
NORM_EPS = 1e-06
CORES = 2
F32 = jnp.float32
BF16 = jnp.bfloat16
VM = pl.BlockSpec(memory_space=pltpu.VMEM)
SM = pl.BlockSpec(memory_space=pltpu.SMEM)


def sds(shape, dtype):
    return jax.ShapeDtypeStruct(shape, dtype)


def dot_nt(a, b):
    return lax.dot_general(a, b, (((1,), (1,)), ((), ())), preferred_element_type=F32)


def dot_nn(a, b):
    return lax.dot_general(a, b, (((1,), (0,)), ((), ())), preferred_element_type=F32)


def prep_kernel(wq, wk, wv, out, *, kv_heads, group, qk):
    chips = out.shape[0]
    rows = out.shape[1] // kv_heads
    parts = chips // (2 * group)
    quarter = qk // 2 // parts
    key_parts = chips // 4
    key_rows = qk // 2 // key_parts
    width = 2 * qk
    val_rows = width // (chips // 2)
    for g in range(kv_heads):
        base = rows * g
        for r in range(group):
            h = g * group + r
            t = wq[:, width * h : width * (h + 1)].astype(F32).T
            for m in range(2):
                for part in range(parts):
                    z = (r * 2 + m) * parts + part
                    lo = qk * m + quarter * part
                    hi = lo + qk // 2
                    out[z, base : base + quarter] = t[lo : lo + quarter].astype(BF16)
                    out[z, base + quarter : base + 2 * quarter] = t[hi : hi + quarter].astype(BF16)
        tk = wk[:, width * g : width * (g + 1)].astype(F32).T
        tv = wv[:, width * g : width * (g + 1)].astype(F32).T
        off = base + 2 * quarter
        for m in range(2):
            for part in range(key_parts):
                lo = qk * m + key_rows * part
                hi = lo + qk // 2
                both = jnp.concatenate([tk[lo : lo + key_rows], tk[hi : hi + key_rows]], axis=0)
                out[m * key_parts + part, off : off + 2 * key_rows] = both.astype(BF16)
        for y in range(chips // 2):
            out[chips // 2 + y, off : off + val_rows] = tv[
                val_rows * y : val_rows * (y + 1)
            ].astype(BF16)


def norm_kernel(tokens, gain, linked, normed, reach, depth):
    x = tokens[...].astype(F32)
    mean = jnp.mean(x * x, axis=-1, keepdims=True)
    normed[...] = (x * lax.rsqrt(mean + NORM_EPS) * gain[...].astype(F32)).astype(BF16)

    @pl.when(pl.program_id(0) == 0)
    def _():
        r = linked[...]
        for _step in range(5):
            r = jnp.minimum(dot_nn(r, r), 1.0).astype(BF16)
        reach[...] = r
        depth[...] = dot_nt(jnp.ones((8, r.shape[1]), BF16), r) - 1.0


def dot_kernel(sc, x, w, keep, send, scr):
    core = sc[0]
    chips, rows, slab = w.shape
    acc = jnp.zeros((rows, x.shape[0]), F32)
    for z in range(chips):
        at = pl.multiple_of((CORES * z + core) * slab, slab)
        acc = acc + dot_nt(w[z], x[:, pl.ds(at, slab)])
    scr[...] = acc
    half = rows // CORES
    keep[...] = scr[pl.ds(pl.multiple_of(half * core, 8), half)]
    send[...] = scr[pl.ds(pl.multiple_of(half * (1 - core), 8), half)]


def rotate_kernel(sc, keep, recv, cos, sin, out, *, quarter, key_rows):
    p = keep[...] + recv[...]
    chips = out.shape[0]
    chip = sc[1]
    at_q = pl.multiple_of(sc[2] * quarter, 8)
    at_k = pl.multiple_of(sc[3] * key_rows, 8)
    cq, sq = cos[pl.ds(at_q, quarter)], sin[pl.ds(at_q, quarter)]
    is_key = chip < chips // 2
    ck = jnp.where(is_key, cos[pl.ds(at_k, key_rows)], 1.0)
    sk = jnp.where(is_key, sin[pl.ds(at_k, key_rows)], 0.0)
    a, c = p[:quarter], p[quarter : 2 * quarter]
    ka = p[2 * quarter : 2 * quarter + key_rows]
    kc = p[2 * quarter + key_rows :]
    turned = jnp.concatenate(
        [a * cq - c * sq, c * cq + a * sq, ka * ck - kc * sk, kc * ck + ka * sk], axis=0
    ).astype(BF16)
    for z in range(chips):
        out[z] = turned


def attend_kernel(sc, recv, reach, ck, cv, *refs, group, qk, quarter, key_rows, aliased):
    if aliased:
        refs = refs[2:]
    ko, vo, acc_out, stat_out, qs, kf, vf = refs
    chips = recv.shape[0]
    parts = chips // (2 * group)
    key_parts = chips // 4
    step = pl.program_id(0)
    per_step = ck.shape[0]
    span = ck.shape[2]
    width = 2 * qk
    proposals = 16
    n_tok = reach.shape[0]

    @pl.when(step == 0)
    def _():
        for r in range(group):
            pieces = []
            for m in range(2):
                v = (r * 2 + m) * parts
                pieces += [recv[v + p, 0:quarter] for p in range(parts)]
                pieces += [recv[v + p, quarter : 2 * quarter] for p in range(parts)]
            qs[r] = jnp.concatenate(pieces, axis=0).astype(F32).T.astype(BF16)
        lo = 2 * quarter
        pieces = []
        for m in range(2):
            both = [recv[m * key_parts + p, lo:].astype(F32) for p in range(key_parts)]
            pieces += [t[:key_rows] for t in both] + [t[key_rows:] for t in both]
        kf[...] = jnp.concatenate(pieces, axis=0).T.astype(BF16)
        pieces = [recv[chips // 2 + y, lo:] for y in range(chips // 2)]
        vf[...] = jnp.concatenate(pieces, axis=0).astype(F32).T.astype(BF16)

    offset = sc[4]
    lane = lax.broadcasted_iota(jnp.int32, (1, width), 1)
    maps = [(lane < qk).astype(F32).astype(BF16), (lane >= qk).astype(F32).astype(BF16)]
    for k in range(per_step):
        b = step * per_step + k
        start = sc[8 + b]
        row0 = pl.multiple_of(b * proposals, proposals)
        shift = offset - start
        touches = (shift < proposals) & (shift + span > 0)
        ko[k, 0] = ck[k, 0]
        vo[k, 0] = cv[k, 0]

        @pl.when(touches)
        def _():
            rel = lax.broadcasted_iota(jnp.int32, (span, n_tok), 0) + shift
            col = lax.broadcasted_iota(jnp.int32, (span, n_tok), 1) - row0
            inside = (rel >= 0) & (rel < proposals)
            onehot = jnp.where(inside & (rel == col), 1.0, 0.0).astype(BF16)
            written = inside[:, :width]
            ko[k, 0] = jnp.where(written, dot_nn(onehot, kf[...]), ck[k, 0].astype(F32)).astype(BF16)
            vo[k, 0] = jnp.where(written, dot_nn(onehot, vf[...]), cv[k, 0].astype(F32)).astype(BF16)

        rel = lax.broadcasted_iota(jnp.int32, (n_tok, span), 1) + shift
        row = lax.broadcasted_iota(jnp.int32, (n_tok, span), 0) - row0
        hot = jnp.where((rel == row) & (row >= 0) & (row < proposals), 1.0, 0.0).astype(BF16)
        in_tree = dot_nn(reach[pl.ds(row0, proposals), :], hot)
        rel16 = lax.broadcasted_iota(jnp.int32, (proposals, span), 1) + shift
        open16 = jnp.where(rel16 < 0, 1.0, in_tree)
        opened = jnp.concatenate([open16] * (2 * group), axis=0) > 0.5
        rows = []
        for rh in range(2):
            for m in range(2):
                for r2 in range(group // 2):
                    rows.append(qs[rh * (group // 2) + r2, pl.ds(row0, proposals), :] * maps[m])
        q = jnp.concatenate(rows, axis=0)
        s = dot_nt(q, ko[k, 0]) * (qk ** (-0.5))
        top = jnp.max(jnp.where(opened, s, NEG_FILL), axis=1, keepdims=True)
        w = jnp.where(opened, jnp.exp(s - top), 0.0)
        total = jnp.sum(w, axis=1, keepdims=True)
        acc_out[k] = dot_nn(w.astype(BF16), vo[k, 0]).astype(BF16)
        lanes = lax.broadcasted_iota(jnp.int32, (q.shape[0], 128), 1)
        stat = jnp.where(lanes == 0, top, jnp.where(lanes == 1, total, 0.0))
        stat_out[k] = stat.T[:8]


def split3(x):
    hi = x.astype(BF16).astype(F32)
    mid = (x - hi).astype(BF16).astype(F32)
    lo = (x - hi - mid).astype(BF16).astype(F32)
    return [hi, mid, lo]


def pair_kernel(acc0, stat0, acc1, stat1, out):
    seqs, rows, _ = acc0.shape
    half = rows // 2
    for b in range(seqs):
        t0, n0 = stat0[b, 0:1], stat0[b, 1:2]
        t1, n1 = stat1[b, 0:1], stat1[b, 1:2]
        top = jnp.maximum(t0, t1)
        e0, e1 = jnp.exp(t0 - top), jnp.exp(t1 - top)
        total = n0 * e0 + n1 * e1
        cols = jnp.concatenate([e0, e1, jnp.zeros((6, rows), F32)], axis=0).T
        acc = acc0[b].astype(F32) * cols[:, 0:1] + acc1[b].astype(F32) * cols[:, 1:2]
        acc = acc.astype(BF16)
        info = jnp.concatenate(split3(top) + split3(total) + [jnp.zeros((2, rows), F32)], axis=0)
        for rh in range(2):
            out[2 * b + rh, 0:half] = acc[half * rh : half * (rh + 1)]
            view = info if rh == 0 else pltpu.roll(info, half, 1)
            out[2 * b + rh, half : half + 8] = view.astype(BF16)


def finish_kernel(lam, recv, gain, out):
    chips, full, _ = recv.shape
    half = full - 8
    tops, totals = [], []
    for s in range(chips):
        info = recv[s, half:].astype(F32)
        tops.append(info[0:1] + info[1:2] + info[2:3])
        totals.append(info[3:4] + info[4:5] + info[5:6])
    tops = jnp.concatenate(tops, axis=0)
    totals = jnp.concatenate(totals, axis=0)
    scale = jnp.exp(tops - jnp.max(tops, axis=0, keepdims=True))
    den = jnp.sum(scale * totals, axis=0, keepdims=True)
    cols = jnp.concatenate([scale, den, jnp.zeros((7, scale.shape[1]), F32)], axis=0).T[:half]
    num = recv[0, 0:half].astype(F32) * cols[:, 0:1]
    for s in range(1, chips):
        num = num + recv[s, 0:half].astype(F32) * cols[:, s : s + 1]
    attended = num / cols[:, chips : chips + 1]
    quarter = half // 2
    row = lax.broadcasted_iota(jnp.int32, (quarter, 1), 0)
    lam_col = jnp.where(row < quarter // 2, lam[0], lam[1])
    diff = attended[:quarter] - lam_col * attended[quarter:]
    mean = jnp.mean(diff * diff, axis=-1, keepdims=True)
    res = (diff * lax.rsqrt(mean + NORM_EPS) * gain[...].astype(F32)).astype(BF16)
    for z in range(chips):
        out[z] = res


def out_kernel(sc, mine, other, w, out, *, group):
    chips, _, v_dim = mine.shape
    core = sc[0]
    total = jnp.zeros((chips // 2 * 16, w.shape[1]), F32)
    for src, g in ((mine, 1 - core), (other, core)):
        for rh in range(2):
            for r2 in range(group // 2):
                x = jnp.concatenate(
                    [src[2 * b + rh, 16 * r2 : 16 * (r2 + 1)] for b in range(chips // 2)], axis=0
                )
                at = pl.multiple_of((g * group + rh * (group // 2) + r2) * v_dim, v_dim)
                total = total + dot_nn(x, w[pl.ds(at, v_dim)])
    res = total.astype(BF16)
    for t in range(out.shape[0]):
        out[t] = res


def sum_kernel(parts, out):
    total = parts[0].astype(F32)
    for t in range(1, parts.shape[0]):
        total = total + parts[t].astype(F32)
    out[...] = total.astype(BF16)


def on_device(
    tokens,
    norm_gain,
    query_weight,
    key_weight,
    value_weight,
    out_weight,
    head_gain,
    mix_lambda,
    cache_keys,
    cache_values,
    lengths,
    accepted,
    parents,
):
    seqs, proposals, width = tokens.shape
    n_tok = seqs * proposals
    local_kv, span = cache_keys.shape[1:3]
    group = mix_lambda.shape[0] // local_kv
    qk = cache_keys.shape[-1] // 2
    v_dim = cache_values.shape[-1]
    shards = lax.axis_size("kv")
    tps = lax.axis_size("tp")
    chips = shards // CORES
    cols = query_weight.shape[1] + key_weight.shape[1] + value_weight.shape[1]
    rows = cols // shards
    parts = chips // (2 * group)
    quarter = qk // 2 // parts
    key_rows = qk // 2 // (chips // 4)
    me = lax.axis_index("kv")
    chip, core = me // CORES, me % CORES
    same_core = [[CORES * z + c for z in range(chips)] for c in range(CORES)]
    pairs = [(i, i ^ 1) for i in range(shards)]

    def over_chips(x):
        return lax.all_to_all(x, "kv", 0, 0, axis_index_groups=same_core, tiled=True)

    def swap(x):
        return lax.ppermute(x, "kv", pairs)

    weights = pl.pallas_call(
        functools.partial(prep_kernel, kv_heads=local_kv, group=group, qk=qk),
        out_shape=sds((chips, cols // chips, query_weight.shape[0]), BF16),
        in_specs=[VM] * 3,
        out_specs=VM,
        name="prep",
    )(query_weight, key_weight, value_weight)
    weights = over_chips(weights)

    starts = lengths + accepted
    tok = jnp.arange(n_tok, dtype=jnp.int32)
    up = parents.reshape(n_tok) + tok // proposals * proposals
    linked = ((up[:, None] == tok[None, :]) & (tok[:, None] % proposals > 0)) | (
        tok[:, None] == tok[None, :]
    )
    blocks = 4
    normed, reach, depth = pl.pallas_call(
        norm_kernel,
        grid=(blocks,),
        out_shape=(
            sds((n_tok, width), BF16),
            sds((n_tok, n_tok), BF16),
            sds((8, n_tok), F32),
        ),
        in_specs=[
            pl.BlockSpec((n_tok // blocks, width), lambda i: (i, 0)),
            pl.BlockSpec((1, width), lambda i: (0, 0)),
            pl.BlockSpec((n_tok, n_tok), lambda i: (0, 0)),
        ],
        out_specs=(
            pl.BlockSpec((n_tok // blocks, width), lambda i: (i, 0)),
            pl.BlockSpec((n_tok, n_tok), lambda i: (0, 0)),
            pl.BlockSpec((8, n_tok), lambda i: (0, 0)),
        ),
        name="norm",
    )(tokens.reshape(n_tok, width), norm_gain.reshape(1, width), linked.astype(BF16))
    position = jnp.repeat(starts, proposals) + depth[0].astype(jnp.int32)
    inverse = ROTARY_BASE ** (-jnp.arange(qk // 2, dtype=F32) / (qk // 2))
    angles = position.astype(F32)[None, :] * inverse[:, None]
    cosine, sine = jnp.cos(angles), jnp.sin(angles)

    scalars = jnp.concatenate(
        [
            jnp.stack(
                [
                    core,
                    chip,
                    chip % parts,
                    chip % (chips // 4),
                    me * span,
                    1 - core,
                    lax.axis_index("tp"),
                    chip,
                ]
            ).astype(jnp.int32),
            starts,
        ]
    )
    keep, send = pl.pallas_call(
        dot_kernel,
        out_shape=(sds((rows, n_tok), F32), sds((rows, n_tok), F32)),
        in_specs=[SM, VM, VM],
        out_specs=(VM, VM),
        scratch_shapes=[pltpu.VMEM((rows * CORES, n_tok), F32)],
        name="project",
    )(scalars, normed, weights)
    projected = pl.pallas_call(
        functools.partial(rotate_kernel, quarter=quarter, key_rows=key_rows),
        out_shape=sds((chips, rows, n_tok), BF16),
        in_specs=[SM, VM, VM, VM, VM],
        out_specs=VM,
        name="turn",
    )(scalars, keep, swap(send), cosine, sine)
    near = over_chips(projected)
    far = swap(near)

    per_step = 2
    stat_shape = (seqs, 8, 2 * group * proposals)

    def attend(head_slot, recv, held):
        aliased = held is not None

        def cache_map(i, sc):
            return (i, sc[head_slot], 0, 0)

        cache_spec = pl.BlockSpec((per_step, 1, span, v_dim), cache_map)
        whole3 = pl.BlockSpec((chips, rows, n_tok), lambda i, sc: (0, 0, 0))
        whole2 = pl.BlockSpec((n_tok, n_tok), lambda i, sc: (0, 0))
        in_specs = [whole3, whole2, cache_spec, cache_spec]
        operands = [recv, reach, cache_keys, cache_values]
        aliases = {}
        if aliased:
            in_specs += [pl.BlockSpec(memory_space=pl.ANY)] * 2
            operands += list(held)
            aliases = {5: 0, 6: 1}
        return pl.pallas_call(
            functools.partial(
                attend_kernel,
                group=group,
                qk=qk,
                quarter=quarter,
                key_rows=key_rows,
                aliased=aliased,
            ),
            grid_spec=pltpu.PrefetchScalarGridSpec(
                num_scalar_prefetch=1,
                grid=(seqs // per_step,),
                in_specs=in_specs,
                out_specs=(
                    cache_spec,
                    cache_spec,
                    pl.BlockSpec(
                        (per_step, 2 * group * proposals, v_dim), lambda i, sc: (i, 0, 0)
                    ),
                    pl.BlockSpec((per_step,) + stat_shape[1:], lambda i, sc: (i, 0, 0)),
                ),
                scratch_shapes=[
                    pltpu.VMEM((group, n_tok, 2 * qk), BF16),
                    pltpu.VMEM((n_tok, 2 * qk), BF16),
                    pltpu.VMEM((n_tok, v_dim), BF16),
                ],
            ),
            out_shape=(
                sds(cache_keys.shape, BF16),
                sds(cache_values.shape, BF16),
                sds((seqs, 2 * group * proposals, v_dim), BF16),
                sds(stat_shape, F32),
            ),
            input_output_aliases=aliases,
            name="attend_far" if aliased else "attend_near",
        )(scalars, *operands)

    keys_half, values_half, acc_near, stat_near = attend(0, near, None)
    acc_in, stat_in = swap(acc_near), swap(stat_near)
    keys_out, values_out, acc_far, stat_far = attend(5, far, (keys_half, values_half))
    half = group * proposals
    pieces = pl.pallas_call(
        pair_kernel,
        out_shape=sds((chips, half + 8, v_dim), BF16),
        in_specs=[VM] * 4,
        out_specs=VM,
        name="pair",
    )(acc_far, stat_far, acc_in, stat_in)
    pieces = over_chips(pieces)
    first_head = (1 - core) * group + (chip % 2) * (group // 2)
    lam = lax.dynamic_slice_in_dim(mix_lambda, first_head, group // 2, 0)
    heads = pl.pallas_call(
        finish_kernel,
        out_shape=sds((chips, half // 2, v_dim), BF16),
        in_specs=[SM, VM, VM],
        out_specs=VM,
        name="finish",
    )(lam, pieces, head_gain.reshape(1, v_dim))
    heads_near = over_chips(heads)
    heads_far = swap(heads_near)
    local_rows = local_kv * group * v_dim
    out_cols = out_weight.shape[1]
    term = pl.pallas_call(
        functools.partial(out_kernel, group=group),
        grid_spec=pltpu.PrefetchScalarGridSpec(
            num_scalar_prefetch=1,
            grid=(1,),
            in_specs=[
                pl.BlockSpec((chips, half // 2, v_dim), lambda i, sc: (0, 0, 0)),
                pl.BlockSpec((chips, half // 2, v_dim), lambda i, sc: (0, 0, 0)),
                pl.BlockSpec((local_rows, out_cols), lambda i, sc: (sc[6], 0)),
            ],
            out_specs=pl.BlockSpec((tps, n_tok, out_cols), lambda i, sc: (0, 0, 0)),
        ),
        out_shape=sds((tps, n_tok, out_cols), BF16),
        name="project_out",
    )(scalars, heads_near, heads_far, out_weight)
    term = lax.all_to_all(term, "tp", 0, 0, tiled=True)
    mixed = pl.pallas_call(
        sum_kernel,
        out_shape=sds((n_tok, out_cols), BF16),
        in_specs=[VM],
        out_specs=VM,
        name="sum_terms",
    )(term)
    return (mixed.reshape(seqs, proposals, out_cols), keys_out, values_out)


def solution(mesh):
    in_specs = (
        P("grp", None, None),
        P(),
        P("kv", "tp"),
        P("kv", "tp"),
        P("kv", "tp"),
        P(None, "kv"),
        P(),
        P("tp"),
        P("grp", "tp", "kv", None),
        P("grp", "tp", "kv", None),
        P("grp"),
        P("grp"),
        P("grp", None),
    )
    out_specs = (P("grp", None, "kv"), P("grp", "tp", "kv", None), P("grp", "tp", "kv", None))
    return jax.shard_map(
        on_device, mesh=mesh, in_specs=in_specs, out_specs=out_specs, check_vma=False
    )
```

time: 283 us -> 166 us (0.59)
  waiting for transfers between devices: 71.7 us -> 24.3 us
  blocking collectives: 93.3 us -> 51.2 us
  Pallas kernels: 0 us -> 33.2 us
  local copies, waits for them, and re-layouts: 34.4 us -> 7.5 us
  other arithmetic: 23.5 us -> 2.85 us
  between operations: 14.6 us -> 0.77 us
  starting transfers between devices: 34.1 us -> 45.4 us
  matrix products: 10.3 us -> 0 us
    all_gather x2 -> x0, blocking collectives: 93.3 us -> none  [the longest x1 48.5 us: on_device(): lax.all_gather(highs[None], 'kv', axis=0, tiled=True)]
    all_to_all x0 -> x3, blocking collectives: none -> 51.2 us  [the longest x2 42 us: over_chips(): lax.all_to_all(x, 'kv', 0, 0, axis_index_groups=same_core, tiled=True)]
    all_to_all x3 -> x2, waiting for transfers between devices: 60.6 us -> 21.9 us  [over_chips(): lax.all_to_all(x, 'kv', 0, 0, axis_index_groups=same_core, tiled=True)]
    pallas_call x0 -> x10, Pallas kernels: none -> 33.2 us  [the longest x2 14.2 us: attend(): pl.pallas_call(functools.partial(attend_kernel, group=group, qk=qk, quart...]
    reduce_sum x7 -> x0, other arithmetic: 18 us -> none  [the longest x1 11.5 us: absorb(): jnp.sum(piece_acc.astype(jnp.float32) * scaling[..., None], axis=0)]
    ppermute x0 -> x5, starting transfers between devices: none -> 14.5 us  [swap(): return lax.ppermute(x, 'kv', pairs)]
    all_gather x1 -> x0, waiting for transfers between devices: 11.1 us -> none  [on_device(): lax.all_gather(sums[None].astype(jnp.float32), 'kv', axis=0, tiled=True)]
    dot_general x14 -> x0, matrix products: 10.3 us -> none  [the longest x1 2.4 us: on_device(): jnp.einsum('bsj,bgjc->bgsc', slot_table, fresh_keys, preferred_element_ty...]
  transfers between devices with their start and end apart: 4 -> 7, of which waited for: 3 -> 5; matrix products, arithmetic and copies ran while one was open for 11% -> 4% of each run, Pallas kernels for 0% -> 7%
where the time goes in v1:
time: 166 us; the launch traced here: 165 us
  blocking collectives  51.2 us (31%)
  starting transfers between devices  45.4 us (27%)
  Pallas kernels  33.2 us (20%)
  waiting for transfers between devices  24.3 us (15%)
  local copies, waits for them, and re-layouts  7.5 us (5%)
  other arithmetic  2.85 us (2%)
    all_to_all x2, blocking collectives, over_chips(): lax.all_to_all(x, 'kv', 0, 0, axis_index_groups=same_core, tiled=True)  42 us
    all_to_all x2, starting transfers between devices, over_chips(): lax.all_to_all(x, 'kv', 0, 0, axis_index_groups=same_core, tiled=True)  30.9 us
    all_to_all x2, waiting for transfers between devices, over_chips(): lax.all_to_all(x, 'kv', 0, 0, axis_index_groups=same_core, tiled=True)  21.9 us
    ppermute x5, starting transfers between devices, swap(): return lax.ppermute(x, 'kv', pairs)  14.5 us
    pallas_call x2, Pallas kernels, attend(): pl.pallas_call(functools.partial(attend_kernel, group=group, qk=qk, quart...  14.2 us
    all_to_all x1, blocking collectives, on_device(): term = lax.all_to_all(term, 'tp', 0, 0, tiled=True)  9.23 us
    pallas_call x1, Pallas kernels, on_device(): pl.pallas_call(norm_kernel, grid=(blocks,), out_shape=(sds((n_tok, width)...  4.48 us
    unnamed x20, local copies, waits for them, and re-layouts  4.08 us
  transfers between devices with their start and end apart: 7, of which 5 were waited for; matrix products, arithmetic and copies ran while one was open for 4% of the time, Pallas kernels for 7%

profile of v1, /device:TPU:33, one launch (start us, length us, event | category | flops | bytes accessed | tf_op | source)
XLA Modules:
  0.0 165.2 jit_solution(2046377998526485123)
XLA Ops:
  0.6 1.9 %prep.1 = bf16[16,96,128]{2,1,0:T(8,128)(2,1)} custom-call(bf16[128,1024]{1,0:T(8,128)(2,1)} %wq.1, bf16[128,256]{1,0:T(8,128)(2,1)} %wk.1, bf16[128,256]{1,0:T(8,128)(2,1)} %wv.1), custom_call_target="tpu_custom_call" | custom-call | tf_op jit(solution)/shard_map/prep/pallas_call | solution.py:309
  2.5 24.5 %all-to-all-start = ((bf16[16,96,128]{2,1,0:T(8,128)(2,1)}), bf16[16,96,128]{2,1,0:T(8,128)(2,1)S(1)}, u32[]{:S(2)}, u32[]{:S(2)}) async-start(bf16[16,96,128]{2,1,0:T(8,128)(2,1)} %prep.1), calls=%async_computation | async-start | bytes 786432 | tf_op jit(solution)/shard_map/all_to_all | solution.py:304
  27.1 0.8 reshape.69
  28.7 1.3 reshape.68.gain
  30.8 4.5 %norm.1 = (bf16[128,4096]{1,0:T(8,128)(2,1)}, bf16[128,128]{1,0:T(8,128)(2,1)}, f32[8,128]{1,0:T(8,128)}) custom-call(bf16[128,4096]{1,0:T(8,128)(2,1)} %bitcast.12, bf16[1,4096]{1,0:T(2,128)(2,1)} %reshape.68.gain, bf16[128,128]{1,0:T(8,128)(2,1)} %fusion.2.linked), custom_call_target="tpu_custom_call" | custom-call | tf_op jit(solution)/shard_map/norm/pallas_call | solution.py:325
  36.5 8.3 %all-to-all-done.w = bf16[16,96,128]{2,1,0:T(8,128)(2,1)S(1)} async-done(((bf16[16,96,128]{2,1,0:T(8,128)(2,1)}), bf16[16,96,128]{2,1,0:T(8,128)(2,1)S(1)}, u32[]{:S(2)}, u32[]{:S(2)}) %all-to-all-start) | async-done | bytes 393248 | tf_op jit(solution)/shard_map/all_to_all | solution.py:304
  45.6 2.4 %project.1 = (f32[48,128]{1,0:T(8,128)}, f32[48,128]{1,0:T(8,128)}) custom-call(s32[16]{0:T(128)} %concatenate.3.sc, bf16[128,4096]{1,0:T(8,128)(2,1)} %get-tuple-element.16.x, bf16[16,96,128]{2,1,0:T(8,128)(2,1)} %copy-done), custom_call_target="tpu_custom_call" | custom-call | tf_op jit(solution)/shard_map/project/pallas_call | solution.py:367
  48.0 6.8 %collective-permute-start = (f32[48,128]{1,0:T(8,128)}, f32[48,128]{1,0:T(8,128)S(1)}, u32[]{:S(2)}, u32[]{:S(2)}) collective-permute-start(f32[48,128]{1,0:T(8,128)} %get-tuple-element.18), channel_id=1, source_target_pairs={{0,4},{4,0},{8,12},{12,8},{16,20},{20,16},{24,28},{28,24},{32,36},... | collective-permute-start | bytes 73736 | tf_op jit(solution)/shard_map/ppermute | solution.py:307
  56.5 1.5 turn.1
  58.0 18.6 %all_to_all.25.recv = bf16[16,48,128]{2,1,0:T(8,128)(2,1)} all-to-all(bf16[16,48,128]{2,1,0:T(8,128)(2,1)} %turn.1), channel_id=1, replica_groups={{0,8,16,24,32,40,48,56,64,72,80,88,96,104,112,120},{4,12,20,28,36,44,52..., dimensions={0} | all-to-all | bytes 393216 | tf_op jit(solution)/shard_map/all_to_all | solution.py:304
  76.6 7.1 %attend_near.1 = (bf16[8,2,512,128]{3,2,1,0:T(8,128)(2,1)}, bf16[8,2,512,128]{3,2,1,0:T(8,128)(2,1)}, bf16[8,128,128]{2,1,0:T(8,128)(2,1)}, f32[8,8,128]{2,1,0:T(8,128)}) custom-call(s32[16]{0:T(128)} %concatenate.3.sc, bf16[16,48,128]{2,1,0:T(8,128)(2,1)} %all_to_all.25.recv, bf16[128,128]{1,0:T(8,128)(2,1)} %get-tuple-element.20.reach, ...), custom_call_target="tpu_custom_call" | custom-call | tf_op jit(solution)/shard_map/attend_near/pallas_call | solution.py:404
  83.8 3.5 %collective-permute-start.2 = (bf16[8,128,128]{2,1,0:T(8,128)(2,1)}, bf16[8,128,128]{2,1,0:T(8,128)(2,1)S(1)}, u32[]{:S(2)}, u32[]{:S(2)}) collective-permute-start(bf16[8,128,128]{2,1,0:T(8,128)(2,1)} %get-tuple-element.25), channel_id=1, source_target_pairs={{0,4},{4,0},{8,12},{12,8},{16,20},{20,16},{24,28},{28,24},{32,36},... | collective-permute-start | bytes 786440 | tf_op jit(solution)/shard_map/ppermute | solution.py:307
  87.8 1.1 collective-permute-done.1.recv
  89.6 7.1 %attend_far.1 = (bf16[8,2,512,128]{3,2,1,0:T(8,128)(2,1)}, bf16[8,2,512,128]{3,2,1,0:T(8,128)(2,1)}, bf16[8,128,128]{2,1,0:T(8,128)(2,1)}, f32[8,8,128]{2,1,0:T(8,128)}) custom-call(s32[16]{0:T(128)} %concatenate.3.sc, bf16[16,48,128]{2,1,0:T(8,128)(2,1)} %copy-done.5, ...), custom_call_target="tpu_custom_call", output_to_operand_aliasing={{0}: (5, {}), {1}: (6, {})} | custom-call | tf_op jit(solution)/shard_map/attend_far/pallas_call | solution.py:404
  97.4 2.4 %pair.1 = bf16[16,72,128]{2,1,0:T(8,128)(2,1)} custom-call(bf16[8,128,128]{2,1,0:T(8,128)(2,1)} %get-tuple-element.23.acc0, f32[8,8,128]{2,1,0:T(8,128)} %get-tuple-element.24.stat0, bf16[8,128,128]{2,1,0:T(8,128)(2,1)} %copy-done.4, f32[8,8,128]{2,1,0:T(8,128)} %copy-done.7), custom_call_target="tpu_custom_call" | custom-call | tf_op jit(solution)/shard_map/pair/pallas_call | solution.py:445
  99.8 6.4 %all-to-all-start.2 = ((bf16[16,72,128]{2,1,0:T(8,128)(2,1)}), bf16[16,72,128]{2,1,0:T(8,128)(2,1)S(1)}, u32[]{:S(2)}, u32[]{:S(2)}) async-start(bf16[16,72,128]{2,1,0:T(8,128)(2,1)} %pair.1), calls=%async_computation.2 | async-start | bytes 589824 | tf_op jit(solution)/shard_map/all_to_all | solution.py:304
  106.8 13.5 %all-to-all-done.2.recv = bf16[16,72,128]{2,1,0:T(8,128)(2,1)S(1)} async-done(((bf16[16,72,128]{2,1,0:T(8,128)(2,1)}), bf16[16,72,128]{2,1,0:T(8,128)(2,1)S(1)}, u32[]{:S(2)}, u32[]{:S(2)}) %all-to-all-start.2) | async-done | bytes 294944 | tf_op jit(solution)/shard_map/all_to_all | solution.py:304
  121.1 2.1 %finish.1 = bf16[16,32,128]{2,1,0:T(8,128)(2,1)} custom-call(f32[2]{0:T(128)} %dynamic_slice.3.lam, bf16[16,72,128]{2,1,0:T(8,128)(2,1)} %copy-done.1, bf16[1,128]{1,0:T(2,128)(2,1)} %bitcast.14), custom_call_target="tpu_custom_call" | custom-call | tf_op jit(solution)/shard_map/finish/pallas_call | solution.py:455
  123.2 23.4 %all_to_all.26.mine = bf16[16,32,128]{2,1,0:T(8,128)(2,1)S(1)} all-to-all(bf16[16,32,128]{2,1,0:T(8,128)(2,1)} %finish.1), channel_id=1, replica_groups={{0,8,16,24,32,40,48,56,64,72,80,88,96,104,112,120},{4,12,20,28,36,44,52..., dimensions={0} | all-to-all | bytes 262144 | tf_op jit(solution)/shard_map/all_to_all | solution.py:304
  146.5 3.6 %collective-permute-start.4 = (bf16[16,32,128]{2,1,0:T(8,128)(2,1)S(1)}, bf16[16,32,128]{2,1,0:T(8,128)(2,1)S(1)}, u32[]{:S(2)}, u32[]{:S(2)}) collective-permute-start(bf16[16,32,128]{2,1,0:T(8,128)(2,1)S(1)} %all_to_all.26.mine), channel_id=1, source_target_pairs={{0,4},{4,0},{8,12},{12,8},{16,20},{20,16},{24,28},{28,24},{32,36},... | collective-permute-start | bytes 393224 | tf_op jit(solution)/shard_map/ppermute | solution.py:307
  150.2 1.0 collective-permute-done.4.other
  151.8 2.6 %project_out.1 = bf16[4,128,128]{2,1,0:T(8,128)(2,1)} custom-call(s32[16]{0:T(128)} %concatenate.3.sc, bf16[16,32,128]{2,1,0:T(8,128)(2,1)} %copy-done.3, bf16[16,32,128]{2,1,0:T(8,128)(2,1)} %copy-done.6, bf16[4096,128]{1,0:T(8,128)(2,1)} %w.1), custom_call_target="tpu_custom_call" | custom-call | tf_op jit(solution)/shard_map/project_out/pallas_call | solution.py:466
  154.4 9.2 %all_to_all.27.parts = bf16[4,128,128]{2,1,0:T(8,128)(2,1)} all-to-all(bf16[4,128,128]{2,1,0:T(8,128)(2,1)} %project_out.1), channel_id=1, replica_groups=mesh['grp'=2,'kv'=32,'tp'=4] {'tp'}, dimensions={0} | all-to-all | bytes 262144 | tf_op jit(solution)/shard_map/all_to_all | solution.py:481
  163.7 1.5 sum_terms.1
  (36 shorter events, 9.1 us)
Async XLA Ops:
  2.5 42.3 %all-to-all-start = ((bf16[16,96,128]{2,1,0:T(8,128)(2,1)}), bf16[16,96,128]{2,1,0:T(8,128)(2,1)S(1)}, u32[]{:S(2)}, u32[]{:S(2)}) async-start(bf16[16,96,128]{2,1,0:T(8,128)(2,1)} %prep.1), calls=%async_computation | async-start | bytes 786432 | tf_op jit(solution)/shard_map/all_to_all | solution.py:304
  44.9 0.7 copy-start
  48.0 7.9 %collective-permute-start = (f32[48,128]{1,0:T(8,128)}, f32[48,128]{1,0:T(8,128)S(1)}, u32[]{:S(2)}, u32[]{:S(2)}) collective-permute-start(f32[48,128]{1,0:T(8,128)} %get-tuple-element.18), channel_id=1, source_target_pairs={{0,4},{4,0},{8,12},{12,8},{16,20},{20,16},{24,28},{28,24},{32,36},... | collective-permute-start | bytes 73736 | tf_op jit(solution)/shard_map/ppermute | solution.py:307
  55.9 0.6 copy-start.8
  76.6 10.6 %copy-start.2 = (bf16[16,48,128]{2,1,0:T(8,128)(2,1)S(1)}, bf16[16,48,128]{2,1,0:T(8,128)(2,1)}, u32[]{:S(2)}) copy-start(bf16[16,48,128]{2,1,0:T(8,128)(2,1)} %all_to_all.25.recv) | copy-start | bytes 589828
  83.8 13.0 %collective-permute-start.2 = (bf16[8,128,128]{2,1,0:T(8,128)(2,1)}, bf16[8,128,128]{2,1,0:T(8,128)(2,1)S(1)}, u32[]{:S(2)}, u32[]{:S(2)}) collective-permute-start(bf16[8,128,128]{2,1,0:T(8,128)(2,1)} %get-tuple-element.25), channel_id=1, source_target_pairs={{0,4},{4,0},{8,12},{12,8},{16,20},{20,16},{24,28},{28,24},{32,36},... | collective-permute-start | bytes 786440 | tf_op jit(solution)/shard_map/ppermute | solution.py:307
  87.3 1.7 collective-permute-start.1
  87.4 9.3 %collective-permute-start.3 = (f32[8,8,128]{2,1,0:T(8,128)}, f32[8,8,128]{2,1,0:T(8,128)S(1)}, u32[]{:S(2)}, u32[]{:S(2)}) collective-permute-start(f32[8,8,128]{2,1,0:T(8,128)} %get-tuple-element.26), channel_id=1, source_target_pairs={{0,4},{4,0},{8,12},{12,8},{16,20},{20,16},{24,28},{28,24},{32,36},... | collective-permute-start | bytes 98312 | tf_op jit(solution)/shard_map/ppermute | solution.py:307
  88.9 0.7 copy-start.5
  89.6 16.6 %copy-start.9 = (f32[8]{0:T(128)S(1)}, f32[8]{0:T(128)}, u32[]{:S(2)}) copy-start(f32[8]{0:T(128)} %param.20) | copy-start | bytes 100
  96.7 0.6 copy-start.7
  96.7 0.7 copy-start.4
  99.8 20.6 %all-to-all-start.2 = ((bf16[16,72,128]{2,1,0:T(8,128)(2,1)}), bf16[16,72,128]{2,1,0:T(8,128)(2,1)S(1)}, u32[]{:S(2)}, u32[]{:S(2)}) async-start(bf16[16,72,128]{2,1,0:T(8,128)(2,1)} %pair.1), calls=%async_computation.2 | async-start | bytes 589824 | tf_op jit(solution)/shard_map/all_to_all | solution.py:304
  120.4 0.7 copy-start.1
  146.5 4.6 %copy-start.3 = (bf16[16,32,128]{2,1,0:T(8,128)(2,1)}, bf16[16,32,128]{2,1,0:T(8,128)(2,1)S(1)}, u32[]{:S(2)}) copy-start(bf16[16,32,128]{2,1,0:T(8,128)(2,1)S(1)} %all_to_all.26.mine) | copy-start | bytes 393220
  146.5 4.6 %collective-permute-start.4 = (bf16[16,32,128]{2,1,0:T(8,128)(2,1)S(1)}, bf16[16,32,128]{2,1,0:T(8,128)(2,1)S(1)}, u32[]{:S(2)}, u32[]{:S(2)}) collective-permute-start(bf16[16,32,128]{2,1,0:T(8,128)(2,1)S(1)} %all_to_all.26.mine), channel_id=1, source_target_pairs={{0,4},{4,0},{8,12},{12,8},{16,20},{20,16},{24,28},{28,24},{32,36},... | collective-permute-start | bytes 393224 | tf_op jit(solution)/shard_map/ppermute | solution.py:307
  151.2 0.6 copy-start.6

commit v2 on v1

v2 whole, which is shorter than its diff:
```python
import functools

import jax
import jax.numpy as jnp
from jax import lax
from jax.experimental import pallas as pl
from jax.experimental.pallas import tpu as pltpu
from jax.sharding import PartitionSpec as P

NEG_FILL = -1e30
ROTARY_BASE = 10000.0
NORM_EPS = 1e-06
CORES = 2
F32 = jnp.float32
BF16 = jnp.bfloat16
VM = pl.BlockSpec(memory_space=pltpu.VMEM)
SM = pl.BlockSpec(memory_space=pltpu.SMEM)


def limit(mib):
    return pltpu.CompilerParams(vmem_limit_bytes=mib << 20)


def sds(shape, dtype):
    return jax.ShapeDtypeStruct(shape, dtype)


def dot_nt(a, b):
    return lax.dot_general(a, b, (((1,), (1,)), ((), ())), preferred_element_type=F32)


def dot_nn(a, b):
    return lax.dot_general(a, b, (((1,), (0,)), ((), ())), preferred_element_type=F32)


def prep_kernel(wq_hbm, wk_hbm, wv_hbm, out, wq, wk, wv, sems, *, kv_heads, group, qk):
    copies = [
        pltpu.make_async_copy(src, dst, sems.at[n])
        for n, (src, dst) in enumerate([(wk_hbm, wk), (wv_hbm, wv), (wq_hbm, wq)])
    ]
    for copy in copies:
        copy.start()
    for copy in copies:
        copy.wait()
    chips = out.shape[0]
    rows = out.shape[1] // kv_heads
    parts = chips // (2 * group)
    quarter = qk // 2 // parts
    key_parts = chips // 4
    key_rows = qk // 2 // key_parts
    width = 2 * qk
    val_rows = width // (chips // 2)
    for g in range(kv_heads):
        base = rows * g
        for r in range(group):
            h = g * group + r
            t = wq[:, width * h : width * (h + 1)].astype(F32).T
            for m in range(2):
                for part in range(parts):
                    z = (r * 2 + m) * parts + part
                    lo = qk * m + quarter * part
                    hi = lo + qk // 2
                    out[z, base : base + quarter] = t[lo : lo + quarter].astype(BF16)
                    out[z, base + quarter : base + 2 * quarter] = t[hi : hi + quarter].astype(BF16)
        tk = wk[:, width * g : width * (g + 1)].astype(F32).T
        tv = wv[:, width * g : width * (g + 1)].astype(F32).T
        off = base + 2 * quarter
        for m in range(2):
            for part in range(key_parts):
                lo = qk * m + key_rows * part
                hi = lo + qk // 2
                both = jnp.concatenate([tk[lo : lo + key_rows], tk[hi : hi + key_rows]], axis=0)
                out[m * key_parts + part, off : off + 2 * key_rows] = both.astype(BF16)
        for y in range(chips // 2):
            out[chips // 2 + y, off : off + val_rows] = tv[
                val_rows * y : val_rows * (y + 1)
            ].astype(BF16)


def norm_kernel(tokens, gain, linked, normed, reach, depth):
    x = tokens[...].astype(F32)
    mean = jnp.mean(x * x, axis=-1, keepdims=True)
    normed[...] = (x * lax.rsqrt(mean + NORM_EPS) * gain[...].astype(F32)).astype(BF16)

    @pl.when(pl.program_id(0) == 0)
    def _():
        r = linked[...]
        for _step in range(5):
            r = jnp.minimum(dot_nn(r, r), 1.0).astype(BF16)
        reach[...] = r
        depth[...] = dot_nt(jnp.ones((8, r.shape[1]), BF16), r) - 1.0


def place():
    me = lax.axis_index("kv")
    return me, lax.div(me, CORES), lax.rem(me, CORES)


def dot_kernel(x, w, keep, send, scr):
    _, _, core = place()
    chips, rows, slab = w.shape
    acc = jnp.zeros((rows, x.shape[0]), F32)
    for z in range(chips):
        at = pl.multiple_of((CORES * z + core) * slab, slab)
        acc = acc + dot_nt(w[z], x[:, pl.ds(at, slab)])
    scr[...] = acc
    half = rows // CORES
    keep[...] = scr[pl.ds(pl.multiple_of(half * core, 8), half)]
    send[...] = scr[pl.ds(pl.multiple_of(half * (1 - core), 8), half)]


def rotate_kernel(keep, recv, table, out, *, quarter, key_rows):
    p = keep[...] + recv[...]
    chips = out.shape[0]
    _, chip, _ = place()
    freqs = table.shape[0] // 2
    at_q = pl.multiple_of(lax.rem(chip, freqs // quarter) * quarter, 8)
    at_k = pl.multiple_of(lax.rem(chip, freqs // key_rows) * key_rows, 8)
    cq, sq = table[pl.ds(at_q, quarter)], table[pl.ds(at_q + freqs, quarter)]
    cos_k, sin_k = table[pl.ds(at_k, key_rows)], table[pl.ds(at_k + freqs, key_rows)]
    is_key = chip < chips // 2
    ck = jnp.where(is_key, cos_k, 1.0)
    sk = jnp.where(is_key, sin_k, 0.0)
    a, c = p[:quarter], p[quarter : 2 * quarter]
    ka = p[2 * quarter : 2 * quarter + key_rows]
    kc = p[2 * quarter + key_rows :]
    turned = jnp.concatenate(
        [a * cq - c * sq, c * cq + a * sq, ka * ck - kc * sk, kc * ck + ka * sk], axis=0
    ).astype(BF16)
    for z in range(chips):
        out[z] = turned


def attend_kernel(
    lengths, accepted, recv, reach, ck, cv, acc_out, stat_out, kf, vf, qs, *, qk, quarter, key_rows, side
):
    chips = recv.shape[0]
    group = qs.shape[0]
    parts = chips // (2 * group)
    key_parts = chips // 4
    seqs, _, span, width = ck.shape
    n_tok = reach.shape[0]
    proposals = n_tok // seqs
    me, _, core = place()
    g = core if side == 0 else 1 - core
    scale = qk ** (-0.5)
    for r in range(group):
        pieces = []
        for m in range(2):
            v = (r * 2 + m) * parts
            pieces += [recv[v + p, 0:quarter] for p in range(parts)]
            pieces += [recv[v + p, quarter : 2 * quarter] for p in range(parts)]
        qs[r] = (jnp.concatenate(pieces, axis=0).astype(F32).T * scale).astype(BF16)
    lo = 2 * quarter
    pieces = []
    for m in range(2):
        both = [recv[m * key_parts + p, lo:].astype(F32) for p in range(key_parts)]
        pieces += [t[:key_rows] for t in both] + [t[key_rows:] for t in both]
    kf[...] = jnp.concatenate(pieces, axis=0).T.astype(BF16)
    pieces = [recv[chips // 2 + y, lo:] for y in range(chips // 2)]
    vf[...] = jnp.concatenate(pieces, axis=0).astype(F32).T.astype(BF16)

    lane = lax.broadcasted_iota(jnp.int32, (1, width), 1)
    maps = [(lane < qk).astype(F32).astype(BF16), (lane >= qk).astype(F32).astype(BF16)]
    n_rows = 2 * group * proposals
    slot = lax.rem(lax.broadcasted_iota(jnp.int32, (proposals, n_tok), 1), proposals)
    cached = lax.broadcasted_iota(jnp.int32, (1, span), 1)
    for b in range(seqs):
        row0 = b * proposals
        shift = me * span - lengths[b] - accepted[b]
        rows = []
        for rh in range(2):
            for m in range(2):
                for r2 in range(group // 2):
                    rows.append(qs[rh * (group // 2) + r2, row0 : row0 + proposals] * maps[m])
        q = jnp.concatenate(rows, axis=0)
        old = dot_nt(q, ck[b, g]) + jnp.where(cached + shift < 0, 0.0, NEG_FILL)
        at = slot - shift
        seen = (reach[row0 : row0 + proposals].astype(F32) > 0.5) & (at >= 0) & (at < span)
        new = dot_nt(q, kf[...]).reshape(2 * group, proposals, n_tok)
        new = (new + jnp.where(seen, 0.0, NEG_FILL)[None]).reshape(n_rows, n_tok)
        top = jnp.maximum(
            jnp.max(old, axis=1, keepdims=True), jnp.max(new, axis=1, keepdims=True)
        )
        base = jnp.maximum(top, 0.5 * NEG_FILL)
        w_old, w_new = jnp.exp(old - base), jnp.exp(new - base)
        total = jnp.sum(w_old, axis=1, keepdims=True) + jnp.sum(w_new, axis=1, keepdims=True)
        acc = dot_nn(w_old.astype(BF16), cv[b, g]) + dot_nn(w_new.astype(BF16), vf[...])
        acc_out[b] = acc.astype(BF16)
        lanes = lax.broadcasted_iota(jnp.int32, (n_rows, 128), 1)
        stat = jnp.where(lanes == 0, top, jnp.where(lanes == 1, total, 0.0))
        stat_out[b] = stat.T[:8]


def store_kernel(lengths, accepted, ck, cv, kn, vn, kfar, vfar, ko, vo):
    me, _, core = place()
    b = pl.program_id(0)
    heads, span, width = ck.shape[1:]
    n_tok = kn.shape[0]
    proposals = n_tok // pl.num_programs(0)
    shift = me * span - lengths[b] - accepted[b]
    ko[...] = ck[...]
    vo[...] = cv[...]

    @pl.when((shift < proposals) & (shift + span > 0))
    def _():
        rel = lax.broadcasted_iota(jnp.int32, (span, n_tok), 0) + shift
        col = lax.broadcasted_iota(jnp.int32, (span, n_tok), 1) - b * proposals
        inside = (rel >= 0) & (rel < proposals)
        onehot = jnp.where(inside & (rel == col), 1.0, 0.0).astype(BF16)
        rel = lax.broadcasted_iota(jnp.int32, (span, width), 0) + shift
        written = (rel >= 0) & (rel < proposals)
        for g in range(heads):
            near = jnp.where(core == g, 1.0, 0.0)
            for fresh_n, fresh_f, old, new in ((kn, kfar, ck, ko), (vn, vfar, cv, vo)):
                fresh = fresh_n[...].astype(F32) * near + fresh_f[...].astype(F32) * (1.0 - near)
                placed = dot_nn(onehot, fresh.astype(BF16))
                new[0, g] = jnp.where(written, placed, old[0, g].astype(F32)).astype(BF16)


def split3(x):
    hi = x.astype(BF16).astype(F32)
    mid = (x - hi).astype(BF16).astype(F32)
    lo = (x - hi - mid).astype(BF16).astype(F32)
    return [hi, mid, lo]


def pair_kernel(acc0, stat0, acc1, stat1, out):
    seqs, rows, _ = acc0.shape
    half = rows // 2
    for b in range(seqs):
        t0, n0 = stat0[b, 0:1], stat0[b, 1:2]
        t1, n1 = stat1[b, 0:1], stat1[b, 1:2]
        top = jnp.maximum(t0, t1)
        e0, e1 = jnp.exp(t0 - top), jnp.exp(t1 - top)
        total = n0 * e0 + n1 * e1
        cols = jnp.concatenate([e0, e1, jnp.zeros((6, rows), F32)], axis=0).T
        acc = acc0[b].astype(F32) * cols[:, 0:1] + acc1[b].astype(F32) * cols[:, 1:2]
        acc = acc.astype(BF16)
        info = jnp.concatenate(split3(top) + split3(total) + [jnp.zeros((2, rows), F32)], axis=0)
        for rh in range(2):
            out[2 * b + rh, 0:half] = acc[half * rh : half * (rh + 1)]
            view = info if rh == 0 else pltpu.roll(info, half, 1)
            out[2 * b + rh, half : half + 8] = view.astype(BF16)


def finish_kernel(lam, recv, gain, out):
    chips, full, _ = recv.shape
    half = full - 8
    tops, totals = [], []
    for s in range(chips):
        info = recv[s, half:].astype(F32)
        tops.append(info[0:1] + info[1:2] + info[2:3])
        totals.append(info[3:4] + info[4:5] + info[5:6])
    tops = jnp.concatenate(tops, axis=0)
    totals = jnp.concatenate(totals, axis=0)
    scale = jnp.exp(tops - jnp.max(tops, axis=0, keepdims=True))
    den = jnp.sum(scale * totals, axis=0, keepdims=True)
    cols = jnp.concatenate([scale, den, jnp.zeros((7, scale.shape[1]), F32)], axis=0).T[:half]
    num = recv[0, 0:half].astype(F32) * cols[:, 0:1]
    for s in range(1, chips):
        num = num + recv[s, 0:half].astype(F32) * cols[:, s : s + 1]
    attended = num / cols[:, chips : chips + 1]
    quarter = half // 2
    row = lax.broadcasted_iota(jnp.int32, (quarter, 1), 0)
    lam_col = jnp.where(row < quarter // 2, lam[0], lam[1])
    diff = attended[:quarter] - lam_col * attended[quarter:]
    mean = jnp.mean(diff * diff, axis=-1, keepdims=True)
    res = (diff * lax.rsqrt(mean + NORM_EPS) * gain[...].astype(F32)).astype(BF16)
    for z in range(chips):
        out[z] = res


def out_kernel(src, held, w, out, *, group, side):
    chips, _, v_dim = src.shape
    total = held[...] if held is not None else None
    _, _, core = place()
    g = 1 - core if side == 0 else core
    for rh in range(2):
        for r2 in range(group // 2):
            x = jnp.concatenate(
                [src[2 * b + rh, 16 * r2 : 16 * (r2 + 1)] for b in range(chips // 2)], axis=0
            )
            at = pl.multiple_of((g * group + rh * (group // 2) + r2) * v_dim, v_dim)
            part = dot_nn(x, w[pl.ds(at, v_dim)])
            total = part if total is None else total + part
    out[...] = total.astype(out.dtype)


def out_near_kernel(tp, src, w, out, *, group):
    out_kernel(src, None, w, out, group=group, side=0)


def out_far_kernel(tp, src, held, w, out, *, group):
    out_kernel(src, held, w, out, group=group, side=1)


def add_kernel(a, b, out):
    out[...] = (a[...].astype(F32) + b[...].astype(F32)).astype(BF16)


def on_device(
    tokens,
    norm_gain,
    query_weight,
    key_weight,
    value_weight,
    out_weight,
    head_gain,
    mix_lambda,
    cache_keys,
    cache_values,
    lengths,
    accepted,
    parents,
):
    seqs, proposals, width = tokens.shape
    n_tok = seqs * proposals
    local_kv, span = cache_keys.shape[1:3]
    group = mix_lambda.shape[0] // local_kv
    qk = cache_keys.shape[-1] // 2
    v_dim = cache_values.shape[-1]
    shards = lax.axis_size("kv")
    tps = lax.axis_size("tp")
    chips = shards // CORES
    cols = query_weight.shape[1] + key_weight.shape[1] + value_weight.shape[1]
    rows = cols // shards
    parts = chips // (2 * group)
    quarter = qk // 2 // parts
    key_rows = qk // 2 // (chips // 4)
    me = lax.axis_index("kv")
    chip, core = me // CORES, me % CORES
    same_core = [[CORES * z + c for z in range(chips)] for c in range(CORES)]
    pairs = [(i, i ^ 1) for i in range(shards)]

    def over_chips(x):
        return lax.all_to_all(x, "kv", 0, 0, axis_index_groups=same_core, tiled=True)

    def swap(x):
        return lax.ppermute(x, "kv", pairs)

    weights = pl.pallas_call(
        functools.partial(prep_kernel, kv_heads=local_kv, group=group, qk=qk),
        out_shape=sds((chips, cols // chips, query_weight.shape[0]), BF16),
        in_specs=[pl.BlockSpec(memory_space=pltpu.HBM)] * 3,
        out_specs=VM,
        scratch_shapes=[
            pltpu.VMEM(query_weight.shape, BF16),
            pltpu.VMEM(key_weight.shape, BF16),
            pltpu.VMEM(value_weight.shape, BF16),
            pltpu.SemaphoreType.DMA((3,)),
        ],
        compiler_params=limit(60),
        name="prep",
    )(query_weight, key_weight, value_weight)
    weights = over_chips(weights)

    starts = lengths + accepted
    tok = jnp.arange(n_tok, dtype=jnp.int32)
    up = parents.reshape(n_tok) + tok // proposals * proposals
    linked = ((up[:, None] == tok[None, :]) & (tok[:, None] % proposals > 0)) | (
        tok[:, None] == tok[None, :]
    )
    blocks = 4
    normed, reach, depth = pl.pallas_call(
        norm_kernel,
        grid=(blocks,),
        out_shape=(
            sds((n_tok, width), BF16),
            sds((n_tok, n_tok), BF16),
            sds((8, n_tok), F32),
        ),
        in_specs=[
            pl.BlockSpec((n_tok // blocks, width), lambda i: (i, 0)),
            pl.BlockSpec((1, width), lambda i: (0, 0)),
            pl.BlockSpec((n_tok, n_tok), lambda i: (0, 0)),
        ],
        out_specs=(
            pl.BlockSpec((n_tok // blocks, width), lambda i: (i, 0)),
            pl.BlockSpec((n_tok, n_tok), lambda i: (0, 0)),
            pl.BlockSpec((8, n_tok), lambda i: (0, 0)),
        ),
        compiler_params=limit(16),
        name="norm",
    )(tokens.reshape(n_tok, width), norm_gain.reshape(1, width), linked.astype(BF16))
    position = jnp.repeat(starts, proposals) + depth[0].astype(jnp.int32)
    inverse = ROTARY_BASE ** (-jnp.arange(qk // 2, dtype=F32) / (qk // 2))
    angles = position.astype(F32)[None, :] * inverse[:, None]
    table = jnp.concatenate([jnp.cos(angles), jnp.sin(angles)], axis=0)
    weights, table = lax.optimization_barrier((weights, table))

    keep, send = pl.pallas_call(
        dot_kernel,
        out_shape=(sds((rows, n_tok), F32), sds((rows, n_tok), F32)),
        in_specs=[VM, VM],
        out_specs=(VM, VM),
        scratch_shapes=[pltpu.VMEM((rows * CORES, n_tok), F32)],
        compiler_params=limit(8),
        name="project",
    )(normed, weights)
    projected = pl.pallas_call(
        functools.partial(rotate_kernel, quarter=quarter, key_rows=key_rows),
        out_shape=sds((chips, rows, n_tok), BF16),
        in_specs=[VM, VM, VM],
        out_specs=VM,
        compiler_params=limit(4),
        name="turn",
    )(keep, swap(send), table)
    near = over_chips(projected)
    far = swap(near)

    n_rows = 2 * group * proposals

    def attend(side, recv):
        return pl.pallas_call(
            functools.partial(
                attend_kernel, qk=qk, quarter=quarter, key_rows=key_rows, side=side
            ),
            in_specs=[SM, SM] + [VM] * 4,
            out_specs=(VM,) * 4,
            out_shape=(
                sds((seqs, n_rows, v_dim), BF16),
                sds((seqs, 8, n_rows), F32),
                sds((n_tok, 2 * qk), BF16),
                sds((n_tok, v_dim), BF16),
            ),
            scratch_shapes=[pltpu.VMEM((group, n_tok, 2 * qk), BF16)],
            compiler_params=limit(16),
            cost_estimate=pl.CostEstimate(
                flops=4 * seqs * n_rows * span * v_dim,
                bytes_accessed=2 * seqs * span * v_dim * 2,
                transcendentals=seqs * n_rows * span,
            ),
            name="attend_far" if side else "attend_near",
        )(lengths, accepted, recv, reach, cache_keys, cache_values)

    acc_near, stat_near, kn, vn = attend(0, near)
    acc_in, stat_in = swap(acc_near), swap(stat_near)
    acc_far, stat_far, kfar, vfar = attend(1, far)
    half = group * proposals
    pieces = pl.pallas_call(
        pair_kernel,
        out_shape=sds((chips, half + 8, v_dim), BF16),
        in_specs=[VM] * 4,
        out_specs=VM,
        compiler_params=limit(8),
        name="pair",
    )(acc_far, stat_far, acc_in, stat_in)
    pieces = over_chips(pieces)
    cache_spec = pl.BlockSpec((1, local_kv, span, v_dim), lambda i: (i, 0, 0, 0))
    fresh_spec = pl.BlockSpec((n_tok, v_dim), lambda i: (0, 0))
    keys_out, values_out = pl.pallas_call(
        store_kernel,
        grid=(seqs,),
        in_specs=[SM, SM, cache_spec, cache_spec] + [fresh_spec] * 4,
        out_specs=(cache_spec, cache_spec),
        out_shape=(sds(cache_keys.shape, BF16), sds(cache_values.shape, BF16)),
        compiler_params=limit(16),
        cost_estimate=pl.CostEstimate(
            flops=4 * seqs * n_rows * span * v_dim,
            bytes_accessed=8 * seqs * local_kv * span * v_dim,
            transcendentals=0,
        ),
        name="store",
    )(lengths, accepted, cache_keys, cache_values, kn, vn, kfar, vfar)
    pieces, keys_out, values_out = lax.optimization_barrier((pieces, keys_out, values_out))
    first_head = (1 - core) * group + (chip % 2) * (group // 2)
    lam = lax.dynamic_slice_in_dim(mix_lambda, first_head, group // 2, 0)
    heads = pl.pallas_call(
        finish_kernel,
        out_shape=sds((chips, half // 2, v_dim), BF16),
        in_specs=[SM, VM, VM],
        out_specs=VM,
        compiler_params=limit(4),
        name="finish",
    )(lam, pieces, head_gain.reshape(1, v_dim))
    heads_near = over_chips(heads)
    heads_far = swap(heads_near)
    local_rows = local_kv * group * v_dim
    out_cols = out_weight.shape[1]
    heads_spec = pl.BlockSpec((chips, half // 2, v_dim), lambda i, tp: (0, 0, 0))
    weight_spec = pl.BlockSpec((local_rows, out_cols), lambda i, tp: (tp[0], 0))
    term_spec = pl.BlockSpec((n_tok, out_cols), lambda i, tp: (0, 0))

    def project_out(body, in_specs, dtype, name, *operands):
        return pl.pallas_call(
            functools.partial(body, group=group),
            grid_spec=pltpu.PrefetchScalarGridSpec(
                num_scalar_prefetch=1, grid=(1,), in_specs=in_specs, out_specs=term_spec
            ),
            out_shape=sds((n_tok, out_cols), dtype),
            compiler_params=limit(4),
            name=name,
        )(lax.axis_index("tp").reshape(1), *operands)

    partial_term = project_out(
        out_near_kernel, [heads_spec, weight_spec], F32, "out_near", heads_near, out_weight
    )
    term = project_out(
        out_far_kernel,
        [heads_spec, term_spec, weight_spec],
        BF16,
        "out_far",
        heads_far,
        partial_term,
        out_weight,
    )

    def add_from(x, hops, name):
        return pl.pallas_call(
            add_kernel,
            out_shape=sds(x.shape, BF16),
            in_specs=[VM] * 2,
            out_specs=VM,
            compiler_params=limit(4),
            name=name,
        )(x, lax.ppermute(x, "tp", hops))

    distance = 1
    while distance < tps:
        pairing = [(t, t // (2 * distance) * 2 * distance + 2 * distance - 1 - t % (2 * distance)) for t in range(tps)]
        term = add_from(term, pairing, "sum_terms")
        distance *= 2
    mixed = term
    return (mixed.reshape(seqs, proposals, out_cols), keys_out, values_out)


def solution(mesh):
    in_specs = (
        P("grp", None, None),
        P(),
        P("kv", "tp"),
        P("kv", "tp"),
        P("kv", "tp"),
        P(None, "kv"),
        P(),
        P("tp"),
        P("grp", "tp", "kv", None),
        P("grp", "tp", "kv", None),
        P("grp"),
        P("grp"),
        P("grp", None),
    )
    out_specs = (P("grp", None, "kv"), P("grp", "tp", "kv", None), P("grp", "tp", "kv", None))
    return jax.shard_map(
        on_device, mesh=mesh, in_specs=in_specs, out_specs=out_specs, check_vma=False
    )
```

time: 166 us -> 146 us (0.88)
  Pallas kernels: 33.2 us -> 18.1 us
  blocking collectives: 51.2 us -> 41.5 us
  starting transfers between devices: 45.4 us -> 49.7 us
    all_to_all x1 -> x0, blocking collectives: 9.23 us -> none  [on_device(): term = lax.all_to_all(term, 'tp', 0, 0, tiled=True)]
    pallas_call x4 -> x7, Pallas kernels: 18.4 us -> 11.7 us  [the longest x2 6.68 us: attend(): pl.pallas_call(functools.partial(attend_kernel, qk=qk, quarter=quarter, k...]
    ppermute x0 -> x2, starting transfers between devices: none -> 4.49 us  [add_from(): lax.ppermute(x, 'tp', hops)]
    pallas_call x1, Pallas kernels: 4.48 us -> 1.52 us  [on_device(): pl.pallas_call(norm_kernel, grid=(blocks,), out_shape=(sds((n_tok, width)...]
    all_to_all x2, waiting for transfers between devices: 21.9 us -> 19 us  [over_chips(): lax.all_to_all(x, 'kv', 0, 0, axis_index_groups=same_core, tiled=True)]
    ppermute x0 -> x2, waiting for transfers between devices: none -> 2.73 us  [add_from(): lax.ppermute(x, 'tp', hops)]
    unnamed x20 -> x28, local copies, waits for them, and re-layouts: 4.08 us -> 6.17 us
    pallas_call x1, Pallas kernels: 2.42 us -> 0.49 us  [on_device(): pl.pallas_call(dot_kernel, out_shape=(sds((rows, n_tok), F32), sds((rows,...]
  transfers between devices with their start and end apart: 7 -> 9, of which waited for: 5 -> 7; matrix products, arithmetic and copies ran while one was open for 4% -> 2% of each run, Pallas kernels for 7% -> 6%
where the time goes in v2:
time: 146 us; the launch traced here: 144 us
  starting transfers between devices  49.7 us (34%)
  blocking collectives  41.5 us (28%)
  waiting for transfers between devices  24.3 us (17%)
  Pallas kernels  18.1 us (12%)
  local copies, waits for them, and re-layouts  7.88 us (5%)
  other arithmetic  1.57 us (1%)
    all_to_all x2, blocking collectives, over_chips(): lax.all_to_all(x, 'kv', 0, 0, axis_index_groups=same_core, tiled=True)  41.5 us
    all_to_all x2, starting transfers between devices, over_chips(): lax.all_to_all(x, 'kv', 0, 0, axis_index_groups=same_core, tiled=True)  30.6 us
    all_to_all x2, waiting for transfers between devices, over_chips(): lax.all_to_all(x, 'kv', 0, 0, axis_index_groups=same_core, tiled=True)  19 us
    ppermute x5, starting transfers between devices, swap(): return lax.ppermute(x, 'kv', pairs)  14.6 us
    pallas_call x2, Pallas kernels, attend(): pl.pallas_call(functools.partial(attend_kernel, qk=qk, quarter=quarter, k...  6.68 us
    unnamed x28, local copies, waits for them, and re-layouts  6.17 us
    ppermute x2, starting transfers between devices, add_from(): lax.ppermute(x, 'tp', hops)  4.49 us
    pallas_call x1, Pallas kernels, on_device(): pl.pallas_call(store_kernel, grid=(seqs,), in_specs=[SM, SM, cache_spec,...  4.05 us
  transfers between devices with their start and end apart: 9, of which 7 were waited for; matrix products, arithmetic and copies ran while one was open for 2% of the time, Pallas kernels for 6%

profile of v2, /device:TPU:33, one launch (start us, length us, event | category | flops | bytes accessed | tf_op | source)
XLA Modules:
  0.0 143.8 jit_solution(515237315919661889)
XLA Ops:
  0.7 2.0 %prep.1 = bf16[16,96,128]{2,1,0:T(8,128)(2,1)} custom-call(bf16[128,1024]{1,0:T(8,128)(2,1)} %wq_hbm.1, bf16[128,256]{1,0:T(8,128)(2,1)} %wk_hbm.1, bf16[128,256]{1,0:T(8,128)(2,1)} %wv_hbm.1), custom_call_target="tpu_custom_call" | custom-call | tf_op jit(solution)/shard_map/prep/pallas_call | solution.py:342
  2.7 24.7 %all-to-all-start = ((bf16[16,96,128]{2,1,0:T(8,128)(2,1)}), bf16[16,96,128]{2,1,0:T(8,128)(2,1)S(1)}, u32[]{:S(2)}, u32[]{:S(2)}) async-start(bf16[16,96,128]{2,1,0:T(8,128)(2,1)} %prep.1), calls=%async_computation | async-start | bytes 786432 | tf_op jit(solution)/shard_map/all_to_all | solution.py:337
  29.8 1.2 copy-done.4
  31.0 1.5 %norm.1 = (bf16[128,4096]{1,0:T(8,128)(2,1)S(1)}, bf16[128,128]{1,0:T(8,128)(2,1)S(1)}, f32[8,128]{1,0:T(8,128)S(1)}) custom-call(bf16[128,4096]{1,0:T(8,128)(2,1)S(1)} %bitcast.6, bf16[1,4096]{1,0:T(2,128)(2,1)S(1)} %reshape.73.gain, bf16[128,128]{1,0:T(8,128)(2,1)S(1)} %fusion.2.linked), custom_call_target="tpu_custom_call" | custom-call | tf_op jit(solution)/shard_map/norm/pallas_call | solution.py:365
  33.8 11.4 %all-to-all-done.w = bf16[16,96,128]{2,1,0:T(8,128)(2,1)S(1)} async-done(((bf16[16,96,128]{2,1,0:T(8,128)(2,1)}), bf16[16,96,128]{2,1,0:T(8,128)(2,1)S(1)}, u32[]{:S(2)}, u32[]{:S(2)}) %all-to-all-start) | async-done | bytes 393248 | tf_op jit(solution)/shard_map/all_to_all | solution.py:337
  45.6 6.9 %collective-permute-start = (f32[48,128]{1,0:T(8,128)S(1)}, f32[48,128]{1,0:T(8,128)S(1)}, u32[]{:S(2)}, u32[]{:S(2)}) collective-permute-start(f32[48,128]{1,0:T(8,128)S(1)} %get-tuple-element.27), channel_id=1, source_target_pairs={{0,4},{4,0},{8,12},{12,8},{16,20},{20,16},{24,28},{28,24},{32,36},... | collective-permute-start | bytes 73736 | tf_op jit(solution)/shard_map/ppermute | solution.py:340
  52.5 0.8 collective-permute-done.recv
  54.2 18.3 %all_to_all.20.recv = bf16[16,48,128]{2,1,0:T(8,128)(2,1)S(1)} all-to-all(bf16[16,48,128]{2,1,0:T(8,128)(2,1)S(1)} %turn.1), channel_id=1, replica_groups={{0,8,16,24,32,40,48,56,64,72,80,88,96,104,112,120},{4,12,20,28,36,44,52..., dimensions={0} | all-to-all | bytes 393216 | tf_op jit(solution)/shard_map/all_to_all | solution.py:337
  73.3 3.3 %attend_near.1 = (bf16[8,128,128]{2,1,0:T(8,128)(2,1)S(1)}, f32[8,8,128]{2,1,0:T(8,128)S(1)}, bf16[128,128]{1,0:T(8,128)(2,1)S(1)}, bf16[128,128]{1,0:T(8,128)(2,1)S(1)}) custom-call(s32[8]{0:T(128)S(1)} %copy-done.10, s32[8]{0:T(128)S(1)} %copy-done.11, bf16[16,48,128]{2,1,0:T(8,128)(2,1)S(1)} %all_to_all.20.recv, bf16[128,128]{1,0:T(8,128)(2,1)S(1)} %copy-done.6, ...), custom_call_target="tpu_custom_call" | custom-call | flops 268435456 | bytes 2097152 | tf_op jit(solution)/shard_map/attend_near/pallas_call | solution.py:415
  76.6 3.5 %collective-permute-start.2 = (bf16[8,128,128]{2,1,0:T(8,128)(2,1)S(1)}, bf16[8,128,128]{2,1,0:T(8,128)(2,1)S(1)}, u32[]{:S(2)}, u32[]{:S(2)}) collective-permute-start(bf16[8,128,128]{2,1,0:T(8,128)(2,1)S(1)} %get-tuple-element.32), channel_id=1, source_target_pairs={{0,4},{4,0},{8,12},{12,8},{16,20},{20,16},{24,28},{28,24},{32,36},... | collective-permute-start | bytes 786440 | tf_op jit(solution)/shard_map/ppermute | solution.py:340
  80.6 0.9 collective-permute-done.1.recv
  81.6 3.3 %attend_far.1 = (bf16[8,128,128]{2,1,0:T(8,128)(2,1)S(1)}, f32[8,8,128]{2,1,0:T(8,128)S(1)}, bf16[128,128]{1,0:T(8,128)(2,1)S(1)}, bf16[128,128]{1,0:T(8,128)(2,1)S(1)}) custom-call(s32[8]{0:T(128)S(1)} %copy-done.10, s32[8]{0:T(128)S(1)} %copy-done.11, bf16[16,48,128]{2,1,0:T(8,128)(2,1)S(1)} %collective-permute-done.1.recv, ...), custom_call_target="tpu_custom_call" | custom-call | flops 268435456 | bytes 2097152 | tf_op jit(solution)/shard_map/attend_far/pallas_call | solution.py:415
  85.5 1.3 pair.1
  86.9 6.0 %all-to-all-start.2 = ((bf16[16,72,128]{2,1,0:T(8,128)(2,1)}), bf16[16,72,128]{2,1,0:T(8,128)(2,1)S(1)}, u32[]{:S(2)}, u32[]{:S(2)}) async-start(bf16[16,72,128]{2,1,0:T(8,128)(2,1)} %pair.1), calls=%async_computation.2 | async-start | bytes 589824 | tf_op jit(solution)/shard_map/all_to_all | solution.py:337
  92.9 1.6 %copy-done.2 = bf16[8,2,512,128]{3,2,1,0:T(8,128)(2,1)S(1)} copy-done((bf16[8,2,512,128]{3,2,1,0:T(8,128)(2,1)S(1)}, bf16[8,2,512,128]{3,2,1,0:T(8,128)(2,1)}, u32[]{:S(2)}) %copy-start.2) | copy-done | bytes 2097176
  95.3 4.0 %store.1 = (bf16[8,2,512,128]{3,2,1,0:T(8,128)(2,1)}, bf16[8,2,512,128]{3,2,1,0:T(8,128)(2,1)}) custom-call(s32[8]{0:T(128)S(1)} %copy-done.10, s32[8]{0:T(128)S(1)} %copy-done.11, bf16[8,2,512,128]{3,2,1,0:T(8,128)(2,1)S(1)} %copy-done, bf16[8,2,512,128]{3,2,1,0:T(8,128)(2,1)S(1)} %copy-done.2, bf16[128,128]{1,0:T(8,128)(2,1)S(1)} %get-tuple-element.34.kn, ...), custom_call_target="tpu_custom_call" | custom-call | flops 268435456 | bytes 8388608 | tf_op jit(solution)/shard_map/store/pallas_call | solution.py:452
  99.3 7.6 %all-to-all-done.2.recv = bf16[16,72,128]{2,1,0:T(8,128)(2,1)S(1)} async-done(((bf16[16,72,128]{2,1,0:T(8,128)(2,1)}), bf16[16,72,128]{2,1,0:T(8,128)(2,1)S(1)}, u32[]{:S(2)}, u32[]{:S(2)}) %all-to-all-start.2) | async-done | bytes 294944 | tf_op jit(solution)/shard_map/all_to_all | solution.py:337
  107.0 1.0 finish.1
  108.0 23.2 %all_to_all.21.src = bf16[16,32,128]{2,1,0:T(8,128)(2,1)S(1)} all-to-all(bf16[16,32,128]{2,1,0:T(8,128)(2,1)S(1)} %finish.1), channel_id=1, replica_groups={{0,8,16,24,32,40,48,56,64,72,80,88,96,104,112,120},{4,12,20,28,36,44,52..., dimensions={0} | all-to-all | bytes 262144 | tf_op jit(solution)/shard_map/all_to_all | solution.py:337
  131.1 3.6 %collective-permute-start.4 = (bf16[16,32,128]{2,1,0:T(8,128)(2,1)S(1)}, bf16[16,32,128]{2,1,0:T(8,128)(2,1)S(1)}, u32[]{:S(2)}, u32[]{:S(2)}) collective-permute-start(bf16[16,32,128]{2,1,0:T(8,128)(2,1)S(1)} %all_to_all.21.src), channel_id=1, source_target_pairs={{0,4},{4,0},{8,12},{12,8},{16,20},{20,16},{24,28},{28,24},{32,36},... | collective-permute-start | bytes 393224 | tf_op jit(solution)/shard_map/ppermute | solution.py:340
  136.0 1.5 %collective-permute-start.5 = (bf16[128,128]{1,0:T(8,128)(2,1)S(1)}, bf16[128,128]{1,0:T(8,128)(2,1)S(1)}, u32[]{:S(2)}, u32[]{:S(2)}) collective-permute-start(bf16[128,128]{1,0:T(8,128)(2,1)S(1)} %out_far.1.a), channel_id=1, source_target_pairs={{0,1},{1,0},{2,3},{3,2},{4,5},{5,4},{6,7},{7,6},{8,9},{9,8},{10,11... | collective-permute-start | bytes 98312 | tf_op jit(solution)/shard_map/ppermute | solution.py:517
  137.4 1.4 collective-permute-done.5.b
  138.9 3.0 %collective-permute-start.6 = (bf16[128,128]{1,0:T(8,128)(2,1)S(1)}, bf16[128,128]{1,0:T(8,128)(2,1)S(1)}, u32[]{:S(2)}, u32[]{:S(2)}) collective-permute-start(bf16[128,128]{1,0:T(8,128)(2,1)S(1)} %sum_terms.2.a), channel_id=1, source_target_pairs={{0,3},{1,2},{2,1},{3,0},{4,7},{5,6},{6,5},{7,4},{8,11},{9,10},{10,... | collective-permute-start | bytes 98312 | tf_op jit(solution)/shard_map/ppermute | solution.py:517
  141.9 1.3 collective-permute-done.6.b
  (50 shorter events, 9.5 us)
Async XLA Ops:
  0.6 71.9 %copy-start.10 = (s32[8]{0:T(128)S(1)}, s32[8]{0:T(128)}, u32[]{:S(2)}) copy-start(s32[8]{0:T(128)} %lengths.5) | copy-start | bytes 100
  0.6 71.9 %copy-start.11 = (s32[8]{0:T(128)S(1)}, s32[8]{0:T(128)}, u32[]{:S(2)}) copy-start(s32[8]{0:T(128)} %accepted.5) | copy-start | bytes 100
  2.6 69.9 %copy-start = (bf16[8,2,512,128]{3,2,1,0:T(8,128)(2,1)S(1)}, bf16[8,2,512,128]{3,2,1,0:T(8,128)(2,1)}, u32[]{:S(2)}) copy-start(bf16[8,2,512,128]{3,2,1,0:T(8,128)(2,1)} %ck.5) | copy-start | bytes 6291460
  2.7 42.5 %all-to-all-start = ((bf16[16,96,128]{2,1,0:T(8,128)(2,1)}), bf16[16,96,128]{2,1,0:T(8,128)(2,1)S(1)}, u32[]{:S(2)}, u32[]{:S(2)}) async-start(bf16[16,96,128]{2,1,0:T(8,128)(2,1)} %prep.1), calls=%async_computation | async-start | bytes 786432 | tf_op jit(solution)/shard_map/all_to_all | solution.py:337
  29.8 1.2 copy-start.4
  32.5 0.6 copy-start.5
  45.1 27.4 %copy-start.1 = (bf16[8,2,512,128]{3,2,1,0:T(8,128)(2,1)S(1)}, bf16[8,2,512,128]{3,2,1,0:T(8,128)(2,1)}, u32[]{:S(2)}) copy-start(bf16[8,2,512,128]{3,2,1,0:T(8,128)(2,1)} %cv.5) | copy-start | bytes 6291460
  45.6 7.8 %collective-permute-start = (f32[48,128]{1,0:T(8,128)S(1)}, f32[48,128]{1,0:T(8,128)S(1)}, u32[]{:S(2)}, u32[]{:S(2)}) collective-permute-start(f32[48,128]{1,0:T(8,128)S(1)} %get-tuple-element.27), channel_id=1, source_target_pairs={{0,4},{4,0},{8,12},{12,8},{16,20},{20,16},{24,28},{28,24},{32,36},... | collective-permute-start | bytes 73736 | tf_op jit(solution)/shard_map/ppermute | solution.py:340
  53.4 0.8 copy-start.7
  72.5 0.8 copy-start.6
  76.6 8.9 %collective-permute-start.2 = (bf16[8,128,128]{2,1,0:T(8,128)(2,1)S(1)}, bf16[8,128,128]{2,1,0:T(8,128)(2,1)S(1)}, u32[]{:S(2)}, u32[]{:S(2)}) collective-permute-start(bf16[8,128,128]{2,1,0:T(8,128)(2,1)S(1)} %get-tuple-element.32), channel_id=1, source_target_pairs={{0,4},{4,0},{8,12},{12,8},{16,20},{20,16},{24,28},{28,24},{32,36},... | collective-permute-start | bytes 786440 | tf_op jit(solution)/shard_map/ppermute | solution.py:340
  80.1 1.4 %collective-permute-start.1 = (bf16[16,48,128]{2,1,0:T(8,128)(2,1)S(1)}, bf16[16,48,128]{2,1,0:T(8,128)(2,1)S(1)}, u32[]{:S(2)}, u32[]{:S(2)}) collective-permute-start(bf16[16,48,128]{2,1,0:T(8,128)(2,1)S(1)} %all_to_all.20.recv), channel_id=1, source_target_pairs={{0,4},{4,0},{8,12},{12,8},{16,20},{20,16},{24,28},{28,24},{32,36},... | collective-permute-start | bytes 589832 | tf_op jit(solution)/shard_map/ppermute | solution.py:340
  80.3 12.6 %copy-start.13 = (f32[8]{0:T(128)S(1)}, f32[8]{0:T(128)}, u32[]{:S(2)}) copy-start(f32[8]{0:T(128)} %param.20) | copy-start | bytes 100
  80.3 5.3 %collective-permute-start.3 = (f32[8,8,128]{2,1,0:T(8,128)S(1)}, f32[8,8,128]{2,1,0:T(8,128)S(1)}, u32[]{:S(2)}, u32[]{:S(2)}) collective-permute-start(f32[8,8,128]{2,1,0:T(8,128)S(1)} %get-tuple-element.33), channel_id=1, source_target_pairs={{0,4},{4,0},{8,12},{12,8},{16,20},{20,16},{24,28},{28,24},{32,36},... | collective-permute-start | bytes 98312 | tf_op jit(solution)/shard_map/ppermute | solution.py:340
  84.9 0.6 copy-start.8
  86.9 20.1 %all-to-all-start.2 = ((bf16[16,72,128]{2,1,0:T(8,128)(2,1)}), bf16[16,72,128]{2,1,0:T(8,128)(2,1)S(1)}, u32[]{:S(2)}, u32[]{:S(2)}) async-start(bf16[16,72,128]{2,1,0:T(8,128)(2,1)} %pair.1), calls=%async_computation.2 | async-start | bytes 589824 | tf_op jit(solution)/shard_map/all_to_all | solution.py:337
  92.9 1.6 %copy-start.2 = (bf16[8,2,512,128]{3,2,1,0:T(8,128)(2,1)S(1)}, bf16[8,2,512,128]{3,2,1,0:T(8,128)(2,1)}, u32[]{:S(2)}) copy-start(bf16[8,2,512,128]{3,2,1,0:T(8,128)(2,1)} %cv.5) | copy-start | bytes 6291460
  94.5 0.8 copy-start.9
  95.3 11.7 %copy-start.12 = (bf16[128]{0:T(256)(128)(2,1)S(1)}, bf16[128]{0:T(256)(128)(2,1)}, u32[]{:S(2)}) copy-start(bf16[128]{0:T(256)(128)(2,1)} %param.19) | copy-start | bytes 772
  95.3 39.5 %copy-start.3 = (bf16[4096,128]{1,0:T(8,128)(2,1)S(1)}, bf16[4096,128]{1,0:T(8,128)(2,1)}, u32[]{:S(2)}) copy-start(bf16[4096,128]{1,0:T(8,128)(2,1)} %w.3) | copy-start | bytes 3145732
  131.1 4.6 %collective-permute-start.4 = (bf16[16,32,128]{2,1,0:T(8,128)(2,1)S(1)}, bf16[16,32,128]{2,1,0:T(8,128)(2,1)S(1)}, u32[]{:S(2)}, u32[]{:S(2)}) collective-permute-start(bf16[16,32,128]{2,1,0:T(8,128)(2,1)S(1)} %all_to_all.21.src), channel_id=1, source_target_pairs={{0,4},{4,0},{8,12},{12,8},{16,20},{20,16},{24,28},{28,24},{32,36},... | collective-permute-start | bytes 393224 | tf_op jit(solution)/shard_map/ppermute | solution.py:340
  136.0 2.9 %collective-permute-start.5 = (bf16[128,128]{1,0:T(8,128)(2,1)S(1)}, bf16[128,128]{1,0:T(8,128)(2,1)S(1)}, u32[]{:S(2)}, u32[]{:S(2)}) collective-permute-start(bf16[128,128]{1,0:T(8,128)(2,1)S(1)} %out_far.1.a), channel_id=1, source_target_pairs={{0,1},{1,0},{2,3},{3,2},{4,5},{5,4},{6,7},{7,6},{8,9},{9,8},{10,11... | collective-permute-start | bytes 98312 | tf_op jit(solution)/shard_map/ppermute | solution.py:517
  138.9 4.3 %collective-permute-start.6 = (bf16[128,128]{1,0:T(8,128)(2,1)S(1)}, bf16[128,128]{1,0:T(8,128)(2,1)S(1)}, u32[]{:S(2)}, u32[]{:S(2)}) collective-permute-start(bf16[128,128]{1,0:T(8,128)(2,1)S(1)} %sum_terms.2.a), channel_id=1, source_target_pairs={{0,3},{1,2},{2,1},{3,0},{4,7},{5,6},{6,5},{7,4},{8,11},{9,10},{10,... | collective-permute-start | bytes 98312 | tf_op jit(solution)/shard_map/ppermute | solution.py:517

commit v3 on v2

--- a/solution.py
+++ b/solution.py
@@ -6,6 +6,7 @@
 from jax.experimental import pallas as pl
 from jax.experimental.pallas import tpu as pltpu
 from jax.sharding import PartitionSpec as P
+
 
 NEG_FILL = -1e30
 ROTARY_BASE = 10000.0
@@ -85,7 +86,7 @@
     @pl.when(pl.program_id(0) == 0)
     def _():
         r = linked[...]
-        for _step in range(5):
+        for _ in range(5):
             r = jnp.minimum(dot_nn(r, r), 1.0).astype(BF16)
         reach[...] = r
         depth[...] = dot_nt(jnp.ones((8, r.shape[1]), BF16), r) - 1.0
@@ -97,43 +98,59 @@
 
 
 def dot_kernel(x, w, keep, send, scr):
-    _, _, core = place()
-    chips, rows, slab = w.shape
-    acc = jnp.zeros((rows, x.shape[0]), F32)
-    for z in range(chips):
-        at = pl.multiple_of((CORES * z + core) * slab, slab)
-        acc = acc + dot_nt(w[z], x[:, pl.ds(at, slab)])
+    block, all_rows, slab = w.shape
+    _, chip, core = place()
+    first = lax.div(chip, block) * block
+    acc = jnp.zeros((all_rows, x.shape[0]), F32)
+    for i in range(block):
+        at = pl.multiple_of((CORES * (first + i) + core) * slab, slab)
+        acc = acc + dot_nt(w[i], x[:, pl.ds(at, slab)])
     scr[...] = acc
-    half = rows // CORES
-    keep[...] = scr[pl.ds(pl.multiple_of(half * core, 8), half)]
-    send[...] = scr[pl.ds(pl.multiple_of(half * (1 - core), 8), half)]
-
-
-def rotate_kernel(keep, recv, table, out, *, quarter, key_rows):
+    rows = all_rows // block // CORES
+    for k in range(block):
+        base = CORES * rows * k
+        keep[rows * k : rows * (k + 1)] = scr[pl.ds(pl.multiple_of(base + rows * core, 8), rows)]
+        send[rows * k : rows * (k + 1)] = scr[
+            pl.ds(pl.multiple_of(base + rows * (1 - core), 8), rows)
+        ]
+
+
+def gather_kernel(keep, recv, out):
     p = keep[...] + recv[...]
-    chips = out.shape[0]
+    for t in range(out.shape[0]):
+        out[t] = p
+
+
+def rotate_kernel(parts, table, out, *, quarter, key_rows):
+    total = parts[0]
+    for t in range(1, parts.shape[0]):
+        total = total + parts[t]
+    block = out.shape[0]
     _, chip, _ = place()
     freqs = table.shape[0] // 2
-    at_q = pl.multiple_of(lax.rem(chip, freqs // quarter) * quarter, 8)
-    at_k = pl.multiple_of(lax.rem(chip, freqs // key_rows) * key_rows, 8)
-    cq, sq = table[pl.ds(at_q, quarter)], table[pl.ds(at_q + freqs, quarter)]
-    cos_k, sin_k = table[pl.ds(at_k, key_rows)], table[pl.ds(at_k + freqs, key_rows)]
-    is_key = chip < chips // 2
-    ck = jnp.where(is_key, cos_k, 1.0)
-    sk = jnp.where(is_key, sin_k, 0.0)
-    a, c = p[:quarter], p[quarter : 2 * quarter]
-    ka = p[2 * quarter : 2 * quarter + key_rows]
-    kc = p[2 * quarter + key_rows :]
-    turned = jnp.concatenate(
-        [a * cq - c * sq, c * cq + a * sq, ka * ck - kc * sk, kc * ck + ka * sk], axis=0
-    ).astype(BF16)
-    for z in range(chips):
-        out[z] = turned
+    is_key = lax.rem(chip, block) < parts.shape[0] // 2
+    rows = total.shape[0] // block
+    for k in range(block):
+        p = total[rows * k : rows * (k + 1)]
+        at_q = k % (freqs // quarter) * quarter
+        at_k = k % (freqs // key_rows) * key_rows
+        cq, sq = table[at_q : at_q + quarter], table[freqs + at_q : freqs + at_q + quarter]
+        ck = jnp.where(is_key, table[at_k : at_k + key_rows], 1.0)
+        sk = jnp.where(is_key, table[freqs + at_k : freqs + at_k + key_rows], 0.0)
+        a, c = p[:quarter], p[quarter : 2 * quarter]
+        ka = p[2 * quarter : 2 * quarter + key_rows]
+        kc = p[2 * quarter + key_rows :]
+        turned = jnp.concatenate(
+            [a * cq - c * sq, c * cq + a * sq, ka * ck - kc * sk, kc * ck + ka * sk], axis=0
+        ).astype(BF16)
+        for t in range(block):
+            out[t, rows * k : rows * (k + 1)] = turned
 
 
 def attend_kernel(
-    lengths, accepted, recv, reach, ck, cv, acc_out, stat_out, kf, vf, qs, *, qk, quarter, key_rows, side
+    lengths, accepted, recv, reach, ck, cv, acc_out, stat_out, fresh, qs, *, qk, quarter, key_rows, side
 ):
+    kf, vf = fresh.at[0], fresh.at[1]
     chips = recv.shape[0]
     group = qs.shape[0]
     parts = chips // (2 * group)
@@ -179,24 +196,23 @@
         seen = (reach[row0 : row0 + proposals].astype(F32) > 0.5) & (at >= 0) & (at < span)
         new = dot_nt(q, kf[...]).reshape(2 * group, proposals, n_tok)
         new = (new + jnp.where(seen, 0.0, NEG_FILL)[None]).reshape(n_rows, n_tok)
-        top = jnp.maximum(
-            jnp.max(old, axis=1, keepdims=True), jnp.max(new, axis=1, keepdims=True)
-        )
-        base = jnp.maximum(top, 0.5 * NEG_FILL)
-        w_old, w_new = jnp.exp(old - base), jnp.exp(new - base)
-        total = jnp.sum(w_old, axis=1, keepdims=True) + jnp.sum(w_new, axis=1, keepdims=True)
-        acc = dot_nn(w_old.astype(BF16), cv[b, g]) + dot_nn(w_new.astype(BF16), vf[...])
+        scores = jnp.concatenate([old, new], axis=1)
+        top = jnp.max(scores, axis=1, keepdims=True)
+        w = jnp.exp(scores - jnp.maximum(top, 0.5 * NEG_FILL))
+        total = jnp.sum(w, axis=1, keepdims=True)
+        w = w.astype(BF16)
+        acc = dot_nn(w[:, :span], cv[b, g]) + dot_nn(w[:, span:], vf[...])
         acc_out[b] = acc.astype(BF16)
         lanes = lax.broadcasted_iota(jnp.int32, (n_rows, 128), 1)
         stat = jnp.where(lanes == 0, top, jnp.where(lanes == 1, total, 0.0))
         stat_out[b] = stat.T[:8]
 
 
-def store_kernel(lengths, accepted, ck, cv, kn, vn, kfar, vfar, ko, vo):
+def store_kernel(lengths, accepted, ck, cv, fresh_near, fresh_far, ko, vo):
     me, _, core = place()
     b = pl.program_id(0)
     heads, span, width = ck.shape[1:]
-    n_tok = kn.shape[0]
+    n_tok = fresh_near.shape[1]
     proposals = n_tok // pl.num_programs(0)
     shift = me * span - lengths[b] - accepted[b]
     ko[...] = ck[...]
@@ -212,8 +228,8 @@
         written = (rel >= 0) & (rel < proposals)
         for g in range(heads):
             near = jnp.where(core == g, 1.0, 0.0)
-            for fresh_n, fresh_f, old, new in ((kn, kfar, ck, ko), (vn, vfar, cv, vo)):
-                fresh = fresh_n[...].astype(F32) * near + fresh_f[...].astype(F32) * (1.0 - near)
+            for n, (old, new) in enumerate(((ck, ko), (cv, vo))):
+                fresh = fresh_near[n].astype(F32) * near + fresh_far[n].astype(F32) * (1.0 - near)
                 placed = dot_nn(onehot, fresh.astype(BF16))
                 new[0, g] = jnp.where(written, placed, old[0, g].astype(F32)).astype(BF16)
 
@@ -333,6 +349,25 @@
     same_core = [[CORES * z + c for z in range(chips)] for c in range(CORES)]
     pairs = [(i, i ^ 1) for i in range(shards)]
 
+    block = 4
+    close = [
+        [CORES * (block * o + i) + c for i in range(block)]
+        for o in range(chips // block)
+        for c in range(CORES)
+    ]
+    spread = [
+        [CORES * (block * o + i) + c for o in range(chips // block)]
+        for i in range(block)
+        for c in range(CORES)
+    ]
+
+    def over_close(x):
+        x = x.reshape(block, -1, x.shape[-1])
+        return lax.all_to_all(x, "kv", 0, 0, axis_index_groups=close, tiled=True)
+
+    def over_spread(x):
+        return lax.all_to_all(x, "kv", 0, 0, axis_index_groups=spread, tiled=True)
+
     def over_chips(x):
         return lax.all_to_all(x, "kv", 0, 0, axis_index_groups=same_core, tiled=True)
 
@@ -353,7 +388,7 @@
         compiler_params=limit(60),
         name="prep",
     )(query_weight, key_weight, value_weight)
-    weights = over_chips(weights)
+    weights = over_close(weights)
 
     starts = lengths + accepted
     tok = jnp.arange(n_tok, dtype=jnp.int32)
@@ -391,22 +426,31 @@
 
     keep, send = pl.pallas_call(
         dot_kernel,
-        out_shape=(sds((rows, n_tok), F32), sds((rows, n_tok), F32)),
+        out_shape=(sds((block * rows, n_tok), F32), sds((block * rows, n_tok), F32)),
         in_specs=[VM, VM],
         out_specs=(VM, VM),
-        scratch_shapes=[pltpu.VMEM((rows * CORES, n_tok), F32)],
+        scratch_shapes=[pltpu.VMEM((block * rows * CORES, n_tok), F32)],
         compiler_params=limit(8),
         name="project",
     )(normed, weights)
+    partial_sums = pl.pallas_call(
+        gather_kernel,
+        out_shape=sds((chips // block, block * rows, n_tok), F32),
+        in_specs=[VM, VM],
+        out_specs=VM,
+        compiler_params=limit(4),
+        name="halves",
+    )(keep, swap(send))
+    partial_sums = over_spread(partial_sums)
     projected = pl.pallas_call(
         functools.partial(rotate_kernel, quarter=quarter, key_rows=key_rows),
-        out_shape=sds((chips, rows, n_tok), BF16),
-        in_specs=[VM, VM, VM],
+        out_shape=sds((block, block * rows, n_tok), BF16),
+        in_specs=[VM, VM],
         out_specs=VM,
         compiler_params=limit(4),
         name="turn",
-    )(keep, swap(send), table)
-    near = over_chips(projected)
+    )(partial_sums, table)
+    near = over_close(projected).reshape(chips, rows, n_tok)
     far = swap(near)
 
     n_rows = 2 * group * proposals
@@ -417,12 +461,11 @@
                 attend_kernel, qk=qk, quarter=quarter, key_rows=key_rows, side=side
             ),
             in_specs=[SM, SM] + [VM] * 4,
-            out_specs=(VM,) * 4,
+            out_specs=(VM,) * 3,
             out_shape=(
                 sds((seqs, n_rows, v_dim), BF16),
                 sds((seqs, 8, n_rows), F32),
-                sds((n_tok, 2 * qk), BF16),
-                sds((n_tok, v_dim), BF16),
+                sds((2, n_tok, v_dim), BF16),
             ),
             scratch_shapes=[pltpu.VMEM((group, n_tok, 2 * qk), BF16)],
             compiler_params=limit(16),
@@ -434,9 +477,9 @@
             name="attend_far" if side else "attend_near",
         )(lengths, accepted, recv, reach, cache_keys, cache_values)
 
-    acc_near, stat_near, kn, vn = attend(0, near)
+    acc_near, stat_near, fresh_near = attend(0, near)
     acc_in, stat_in = swap(acc_near), swap(stat_near)
-    acc_far, stat_far, kfar, vfar = attend(1, far)
+    acc_far, stat_far, fresh_far = attend(1, far)
     half = group * proposals
     pieces = pl.pallas_call(
         pair_kernel,
@@ -448,11 +491,11 @@
     )(acc_far, stat_far, acc_in, stat_in)
     pieces = over_chips(pieces)
     cache_spec = pl.BlockSpec((1, local_kv, span, v_dim), lambda i: (i, 0, 0, 0))
-    fresh_spec = pl.BlockSpec((n_tok, v_dim), lambda i: (0, 0))
+    fresh_spec = pl.BlockSpec((2, n_tok, v_dim), lambda i: (0, 0, 0))
     keys_out, values_out = pl.pallas_call(
         store_kernel,
         grid=(seqs,),
-        in_specs=[SM, SM, cache_spec, cache_spec] + [fresh_spec] * 4,
+        in_specs=[SM, SM, cache_spec, cache_spec, fresh_spec, fresh_spec],
         out_specs=(cache_spec, cache_spec),
         out_shape=(sds(cache_keys.shape, BF16), sds(cache_values.shape, BF16)),
         compiler_params=limit(16),
@@ -462,7 +505,7 @@
             transcendentals=0,
         ),
         name="store",
-    )(lengths, accepted, cache_keys, cache_values, kn, vn, kfar, vfar)
+    )(lengths, accepted, cache_keys, cache_values, fresh_near, fresh_far)
     pieces, keys_out, values_out = lax.optimization_barrier((pieces, keys_out, values_out))
     first_head = (1 - core) * group + (chip % 2) * (group // 2)
     lam = lax.dynamic_slice_in_dim(mix_lambda, first_head, group // 2, 0)
@@ -482,7 +525,7 @@
     weight_spec = pl.BlockSpec((local_rows, out_cols), lambda i, tp: (tp[0], 0))
     term_spec = pl.BlockSpec((n_tok, out_cols), lambda i, tp: (0, 0))
 
-    def project_out(body, in_specs, dtype, name, *operands):
+    def project_out(body, in_specs, dtype, *operands):
         return pl.pallas_call(
             functools.partial(body, group=group),
             grid_spec=pltpu.PrefetchScalarGridSpec(
@@ -490,36 +533,33 @@
             ),
             out_shape=sds((n_tok, out_cols), dtype),
             compiler_params=limit(4),
-            name=name,
         )(lax.axis_index("tp").reshape(1), *operands)
 
     partial_term = project_out(
-        out_near_kernel, [heads_spec, weight_spec], F32, "out_near", heads_near, out_weight
+        out_near_kernel, [heads_spec, weight_spec], F32, heads_near, out_weight
     )
     term = project_out(
         out_far_kernel,
         [heads_spec, term_spec, weight_spec],
         BF16,
-        "out_far",
         heads_far,
         partial_term,
         out_weight,
     )
 
-    def add_from(x, hops, name):
+    def add_from(x, hops):
         return pl.pallas_call(
             add_kernel,
             out_shape=sds(x.shape, BF16),
             in_specs=[VM] * 2,
             out_specs=VM,
             compiler_params=limit(4),
-            name=name,
         )(x, lax.ppermute(x, "tp", hops))
 
     distance = 1
     while distance < tps:
         pairing = [(t, t // (2 * distance) * 2 * distance + 2 * distance - 1 - t % (2 * distance)) for t in range(tps)]
-        term = add_from(term, pairing, "sum_terms")
+        term = add_from(term, pairing)
         distance *= 2
     mixed = term
     return (mixed.reshape(seqs, proposals, out_cols), keys_out, values_out)

time: 146 us -> 149 us (1.021)
  blocking collectives: 41.5 us -> 64.9 us
  starting transfers between devices: 49.7 us -> 40.3 us
  waiting for transfers between devices: 24.3 us -> 15.4 us
    all_to_all x0 -> x2, blocking collectives: none -> 41.8 us  [the longest x1 31.1 us: over_spread(): return lax.all_to_all(x, 'kv', 0, 0, axis_index_groups=spread, tiled=True)]
    all_to_all x2 -> x1, starting transfers between devices: 30.6 us -> 4.34 us  [over_chips(): lax.all_to_all(x, 'kv', 0, 0, axis_index_groups=same_core, tiled=True)]
    all_to_all x2 -> x1, blocking collectives: 41.5 us -> 23.2 us  [over_chips(): lax.all_to_all(x, 'kv', 0, 0, axis_index_groups=same_core, tiled=True)]
    all_to_all x2 -> x1, waiting for transfers between devices: 19 us -> 7.53 us  [over_chips(): lax.all_to_all(x, 'kv', 0, 0, axis_index_groups=same_core, tiled=True)]
    all_to_all x0 -> x1, starting transfers between devices: none -> 9.03 us  [over_close(): return lax.all_to_all(x, 'kv', 0, 0, axis_index_groups=close, tiled=True)]
    ppermute x5, starting transfers between devices: 14.6 us -> 22.4 us  [swap(): return lax.ppermute(x, 'kv', pairs)]
    all_to_all x0 -> x1, waiting for transfers between devices: none -> 2.5 us  [over_close(): return lax.all_to_all(x, 'kv', 0, 0, axis_index_groups=close, tiled=True)]
    unnamed x28 -> x30, local copies, waits for them, and re-layouts: 6.17 us -> 5.1 us
where the time goes in v3:
time: 149 us; the launch traced here: 148 us
  blocking collectives  64.9 us (44%)
  starting transfers between devices  40.3 us (27%)
  Pallas kernels  17.9 us (12%)
  waiting for transfers between devices  15.4 us (10%)
  local copies, waits for them, and re-layouts  6.81 us (5%)
  other arithmetic  1.57 us (1%)
    all_to_all x1, blocking collectives, over_spread(): return lax.all_to_all(x, 'kv', 0, 0, axis_index_groups=spread, tiled=True)  31.1 us
    all_to_all x1, blocking collectives, over_chips(): lax.all_to_all(x, 'kv', 0, 0, axis_index_groups=same_core, tiled=True)  23.2 us
    ppermute x5, starting transfers between devices, swap(): return lax.ppermute(x, 'kv', pairs)  22.4 us
    all_to_all x1, blocking collectives, over_close(): return lax.all_to_all(x, 'kv', 0, 0, axis_index_groups=close, tiled=True)  10.7 us
    all_to_all x1, starting transfers between devices, over_close(): return lax.all_to_all(x, 'kv', 0, 0, axis_index_groups=close, tiled=True)  9.03 us
    all_to_all x1, waiting for transfers between devices, over_chips(): lax.all_to_all(x, 'kv', 0, 0, axis_index_groups=same_core, tiled=True)  7.53 us
    pallas_call x2, Pallas kernels, attend(): pl.pallas_call(functools.partial(attend_kernel, qk=qk, quarter=quarter, k...  6.58 us
    unnamed x30, local copies, waits for them, and re-layouts  5.1 us
  transfers between devices with their start and end apart: 9, of which 7 were waited for; matrix products, arithmetic and copies ran while one was open for 2% of the time, Pallas kernels for 6%

profile of v3, /device:TPU:33, one launch (start us, length us, event | category | flops | bytes accessed | tf_op | source)
XLA Modules:
  0.0 147.8 jit_solution(15724622995188913958)
XLA Ops:
  0.6 2.0 %prep.1 = bf16[16,96,128]{2,1,0:T(8,128)(2,1)} custom-call(bf16[128,1024]{1,0:T(8,128)(2,1)} %wq_hbm.1, bf16[128,256]{1,0:T(8,128)(2,1)} %wk_hbm.1, bf16[128,256]{1,0:T(8,128)(2,1)} %wv_hbm.1), custom_call_target="tpu_custom_call" | custom-call | tf_op jit(solution)/shard_map/prep/pallas_call | solution.py:377
  2.7 9.0 %all-to-all-start = ((bf16[4,384,128]{2,1,0:T(8,128)(2,1)}), bf16[4,384,128]{2,1,0:T(8,128)(2,1)S(1)}, u32[]{:S(2)}, u32[]{:S(2)}) async-start(bf16[4,384,128]{2,1,0:T(8,128)(2,1)} %bitcast.12), calls=%async_computation | async-start | bytes 786432 | tf_op jit(solution)/shard_map/all_to_all | solution.py:366
  14.2 1.5 %norm.1 = (bf16[128,4096]{1,0:T(8,128)(2,1)S(1)}, bf16[128,128]{1,0:T(8,128)(2,1)S(1)}, f32[8,128]{1,0:T(8,128)S(1)}) custom-call(bf16[128,4096]{1,0:T(8,128)(2,1)S(1)} %bitcast.8, bf16[1,4096]{1,0:T(2,128)(2,1)S(1)} %reshape.79.gain, bf16[128,128]{1,0:T(8,128)(2,1)S(1)} %fusion.2.linked), custom_call_target="tpu_custom_call" | custom-call | tf_op jit(solution)/shard_map/norm/pallas_call | solution.py:400
  17.0 2.5 %all-to-all-done.w = bf16[4,384,128]{2,1,0:T(8,128)(2,1)S(1)} async-done(((bf16[4,384,128]{2,1,0:T(8,128)(2,1)}), bf16[4,384,128]{2,1,0:T(8,128)(2,1)S(1)}, u32[]{:S(2)}, u32[]{:S(2)}) %all-to-all-start) | async-done | bytes 393248 | tf_op jit(solution)/shard_map/all_to_all | solution.py:366
  19.8 15.1 %collective-permute-start = (f32[192,128]{1,0:T(8,128)S(1)}, f32[192,128]{1,0:T(8,128)S(1)}, u32[]{:S(2)}, u32[]{:S(2)}) collective-permute-start(f32[192,128]{1,0:T(8,128)S(1)} %get-tuple-element.25), channel_id=1, source_target_pairs={{0,4},{4,0},{8,12},{12,8},{16,20},{20,16},{24,28},{28,24},{32,36},... | collective-permute-start | bytes 294920 | tf_op jit(solution)/shard_map/ppermute | solution.py:375
  34.9 0.9 collective-permute-done.recv
  35.8 31.1 %all_to_all.25.parts = f32[4,192,128]{2,1,0:T(8,128)S(1)} all-to-all(f32[4,192,128]{2,1,0:T(8,128)S(1)} %halves.1), channel_id=1, replica_groups={{0,32,64,96},{4,36,68,100},{8,40,72,104},{12,44,76,108},{16,48,80,112},..., dimensions={0} | all-to-all | bytes 786432 | tf_op jit(solution)/shard_map/all_to_all | solution.py:369
  67.0 10.7 %all_to_all.26 = bf16[4,192,128]{2,1,0:T(8,128)(2,1)S(1)} all-to-all(bf16[4,192,128]{2,1,0:T(8,128)(2,1)S(1)} %turn.1), channel_id=1, replica_groups={{0,8,16,24},{4,12,20,28},{32,40,48,56},{36,44,52,60},{64,72,80,88},{68,..., dimensions={0} | all-to-all | bytes 393216 | tf_op jit(solution)/shard_map/all_to_all | solution.py:366
  77.7 1.6 %copy-done.1 = bf16[8,2,512,128]{3,2,1,0:T(8,128)(2,1)S(1)} copy-done((bf16[8,2,512,128]{3,2,1,0:T(8,128)(2,1)S(1)}, bf16[8,2,512,128]{3,2,1,0:T(8,128)(2,1)}, u32[]{:S(2)}) %copy-start.1) | copy-done | bytes 2097176
  79.3 3.3 %attend_near.1 = (bf16[8,128,128]{2,1,0:T(8,128)(2,1)S(1)}, f32[8,8,128]{2,1,0:T(8,128)S(1)}, bf16[2,128,128]{2,1,0:T(8,128)(2,1)S(1)}) custom-call(s32[8]{0:T(128)S(1)} %copy-done.11, s32[8]{0:T(128)S(1)} %copy-done.12, bf16[16,48,128]{2,1,0:T(8,128)(2,1)S(1)} %bitcast.9, bf16[128,128]{1,0:T(8,128)(2,1)S(1)} %copy-done.7, ...), custom_call_target="tpu_custom_call" | custom-call | flops 268435456 | bytes 2097152 | tf_op jit(solution)/shard_map/attend_near/pallas_call | solution.py:459
  82.6 3.2 %collective-permute-start.2 = (bf16[8,128,128]{2,1,0:T(8,128)(2,1)S(1)}, bf16[8,128,128]{2,1,0:T(8,128)(2,1)S(1)}, u32[]{:S(2)}, u32[]{:S(2)}) collective-permute-start(bf16[8,128,128]{2,1,0:T(8,128)(2,1)S(1)} %get-tuple-element.30), channel_id=1, source_target_pairs={{0,4},{4,0},{8,12},{12,8},{16,20},{20,16},{24,28},{28,24},{32,36},... | collective-permute-start | bytes 786440 | tf_op jit(solution)/shard_map/ppermute | solution.py:375
  87.2 3.3 %attend_far.1 = (bf16[8,128,128]{2,1,0:T(8,128)(2,1)S(1)}, f32[8,8,128]{2,1,0:T(8,128)S(1)}, bf16[2,128,128]{2,1,0:T(8,128)(2,1)S(1)}) custom-call(s32[8]{0:T(128)S(1)} %copy-done.11, s32[8]{0:T(128)S(1)} %copy-done.12, bf16[16,48,128]{2,1,0:T(8,128)(2,1)S(1)} %collective-permute-done.1.recv, bf16[128,128]{1,0:T(8,128)(2,1)S(1)} %copy-done.7, ...), custom_call_target="tpu_custom_call" | custom-call | flops 268435456 | bytes 2097152 | tf_op jit(solution)/shard_map/attend_far/pallas_call | solution.py:459
  91.1 1.3 pair.1
  92.4 4.3 %all-to-all-start.3 = ((bf16[16,72,128]{2,1,0:T(8,128)(2,1)}), bf16[16,72,128]{2,1,0:T(8,128)(2,1)S(1)}, u32[]{:S(2)}, u32[]{:S(2)}) async-start(bf16[16,72,128]{2,1,0:T(8,128)(2,1)} %pair.1), calls=%async_computation.3 | async-start | bytes 589824 | tf_op jit(solution)/shard_map/all_to_all | solution.py:372
  96.9 1.6 %copy-done.3 = bf16[8,2,512,128]{3,2,1,0:T(8,128)(2,1)S(1)} copy-done((bf16[8,2,512,128]{3,2,1,0:T(8,128)(2,1)S(1)}, bf16[8,2,512,128]{3,2,1,0:T(8,128)(2,1)}, u32[]{:S(2)}) %copy-start.3) | copy-done | bytes 2097176
  99.3 4.0 %store.1 = (bf16[8,2,512,128]{3,2,1,0:T(8,128)(2,1)}, bf16[8,2,512,128]{3,2,1,0:T(8,128)(2,1)}) custom-call(s32[8]{0:T(128)S(1)} %copy-done.11, s32[8]{0:T(128)S(1)} %copy-done.12, bf16[8,2,512,128]{3,2,1,0:T(8,128)(2,1)S(1)} %copy-done, bf16[8,2,512,128]{3,2,1,0:T(8,128)(2,1)S(1)} %copy-done.3, bf16[2,128,128]{2,1,0:T(8,128)(2,1)S(1)} %get-tuple-element.32.fresh_near, ...), custom_call_target="tpu_custom_call" | custom-call | flops 268435456 | bytes 8388608 | tf_op jit(solution)/shard_map/store/pallas_call | solution.py:495
  103.4 7.5 %all-to-all-done.3.recv = bf16[16,72,128]{2,1,0:T(8,128)(2,1)S(1)} async-done(((bf16[16,72,128]{2,1,0:T(8,128)(2,1)}), bf16[16,72,128]{2,1,0:T(8,128)(2,1)S(1)}, u32[]{:S(2)}, u32[]{:S(2)}) %all-to-all-start.3) | async-done | bytes 294944 | tf_op jit(solution)/shard_map/all_to_all | solution.py:372
  110.9 1.0 finish.1
  111.9 23.2 %all_to_all.27.src = bf16[16,32,128]{2,1,0:T(8,128)(2,1)S(1)} all-to-all(bf16[16,32,128]{2,1,0:T(8,128)(2,1)S(1)} %finish.1), channel_id=1, replica_groups={{0,8,16,24,32,40,48,56,64,72,80,88,96,104,112,120},{4,12,20,28,36,44,52..., dimensions={0} | all-to-all | bytes 262144 | tf_op jit(solution)/shard_map/all_to_all | solution.py:372
  135.1 3.6 %collective-permute-start.4 = (bf16[16,32,128]{2,1,0:T(8,128)(2,1)S(1)}, bf16[16,32,128]{2,1,0:T(8,128)(2,1)S(1)}, u32[]{:S(2)}, u32[]{:S(2)}) collective-permute-start(bf16[16,32,128]{2,1,0:T(8,128)(2,1)S(1)} %all_to_all.27.src), channel_id=1, source_target_pairs={{0,4},{4,0},{8,12},{12,8},{16,20},{20,16},{24,28},{28,24},{32,36},... | collective-permute-start | bytes 393224 | tf_op jit(solution)/shard_map/ppermute | solution.py:375
  139.9 1.5 collective-permute-start.5
  141.4 1.4 collective-permute-done.5.b
  142.8 3.0 %collective-permute-start.6 = (bf16[128,128]{1,0:T(8,128)(2,1)S(1)}, bf16[128,128]{1,0:T(8,128)(2,1)S(1)}, u32[]{:S(2)}, u32[]{:S(2)}) collective-permute-start(bf16[128,128]{1,0:T(8,128)(2,1)S(1)} %shard_map.150.a), channel_id=1, source_target_pairs={{0,3},{1,2},{2,1},{3,0},{4,7},{5,6},{6,5},{7,4},{8,11},{9,10},{10,... | collective-permute-start | bytes 98312 | tf_op jit(solution)/shard_map/ppermute | solution.py:557
  145.8 1.3 collective-permute-done.6.b
  (54 shorter events, 8.8 us)
Async XLA Ops:
  0.6 13.5 %copy-start.5 = (bf16[8,16,4096]{2,1,0:T(8,128)(2,1)S(1)}, bf16[8,16,4096]{2,1,0:T(8,128)(2,1)}, u32[]{:S(2)}) copy-start(bf16[8,16,4096]{2,1,0:T(8,128)(2,1)} %param.13) | copy-start | bytes 3145732
  2.7 16.8 %all-to-all-start = ((bf16[4,384,128]{2,1,0:T(8,128)(2,1)}), bf16[4,384,128]{2,1,0:T(8,128)(2,1)S(1)}, u32[]{:S(2)}, u32[]{:S(2)}) async-start(bf16[4,384,128]{2,1,0:T(8,128)(2,1)} %bitcast.12), calls=%async_computation | async-start | bytes 786432 | tf_op jit(solution)/shard_map/all_to_all | solution.py:366
  15.7 0.6 copy-start.6
  15.7 61.9 %copy-start = (bf16[8,2,512,128]{3,2,1,0:T(8,128)(2,1)S(1)}, bf16[8,2,512,128]{3,2,1,0:T(8,128)(2,1)}, u32[]{:S(2)}) copy-start(bf16[8,2,512,128]{3,2,1,0:T(8,128)(2,1)} %ck.5) | copy-start | bytes 6291460
  15.7 61.9 %copy-start.11 = (s32[8]{0:T(128)S(1)}, s32[8]{0:T(128)}, u32[]{:S(2)}) copy-start(s32[8]{0:T(128)} %lengths.5) | copy-start | bytes 100
  15.8 61.9 %copy-start.12 = (s32[8]{0:T(128)S(1)}, s32[8]{0:T(128)}, u32[]{:S(2)}) copy-start(s32[8]{0:T(128)} %accepted.5) | copy-start | bytes 100
  19.5 47.5 %copy-start.8 = (f32[64,128]{1,0:T(8,128)S(1)}, f32[64,128]{1,0:T(8,128)}, u32[]{:S(2)}) copy-start(f32[64,128]{1,0:T(8,128)} %pad_maximum_fusion.table) | copy-start | bytes 98308
  19.5 58.2 %copy-start.7 = (bf16[128,128]{1,0:T(8,128)(2,1)S(1)}, bf16[128,128]{1,0:T(8,128)(2,1)}, u32[]{:S(2)}) copy-start(bf16[128,128]{1,0:T(8,128)(2,1)} %copy-done.6) | copy-start | bytes 98308
  19.8 16.0 %collective-permute-start = (f32[192,128]{1,0:T(8,128)S(1)}, f32[192,128]{1,0:T(8,128)S(1)}, u32[]{:S(2)}, u32[]{:S(2)}) collective-permute-start(f32[192,128]{1,0:T(8,128)S(1)} %get-tuple-element.25), channel_id=1, source_target_pairs={{0,4},{4,0},{8,12},{12,8},{16,20},{20,16},{24,28},{28,24},{32,36},... | collective-permute-start | bytes 294920 | tf_op jit(solution)/shard_map/ppermute | solution.py:375
  77.7 1.6 %copy-start.1 = (bf16[8,2,512,128]{3,2,1,0:T(8,128)(2,1)S(1)}, bf16[8,2,512,128]{3,2,1,0:T(8,128)(2,1)}, u32[]{:S(2)}) copy-start(bf16[8,2,512,128]{3,2,1,0:T(8,128)(2,1)} %cv.5) | copy-start | bytes 6291460
  79.3 7.9 %copy-start.2 = (bf16[8,2,512,128]{3,2,1,0:T(8,128)(2,1)S(1)}, bf16[8,2,512,128]{3,2,1,0:T(8,128)(2,1)}, u32[]{:S(2)}) copy-start(bf16[8,2,512,128]{3,2,1,0:T(8,128)(2,1)} %cv.5) | copy-start | bytes 6291460
  82.6 8.6 %collective-permute-start.2 = (bf16[8,128,128]{2,1,0:T(8,128)(2,1)S(1)}, bf16[8,128,128]{2,1,0:T(8,128)(2,1)S(1)}, u32[]{:S(2)}, u32[]{:S(2)}) collective-permute-start(bf16[8,128,128]{2,1,0:T(8,128)(2,1)S(1)} %get-tuple-element.30), channel_id=1, source_target_pairs={{0,4},{4,0},{8,12},{12,8},{16,20},{20,16},{24,28},{28,24},{32,36},... | collective-permute-start | bytes 786440 | tf_op jit(solution)/shard_map/ppermute | solution.py:375
  85.7 1.4 collective-permute-start.1
  85.9 10.9 %copy-start.14 = (f32[8]{0:T(128)S(1)}, f32[8]{0:T(128)}, u32[]{:S(2)}) copy-start(f32[8]{0:T(128)} %param.20) | copy-start | bytes 100
  85.9 5.2 %collective-permute-start.3 = (f32[8,8,128]{2,1,0:T(8,128)S(1)}, f32[8,8,128]{2,1,0:T(8,128)S(1)}, u32[]{:S(2)}, u32[]{:S(2)}) collective-permute-start(f32[8,8,128]{2,1,0:T(8,128)S(1)} %get-tuple-element.31), channel_id=1, source_target_pairs={{0,4},{4,0},{8,12},{12,8},{16,20},{20,16},{24,28},{28,24},{32,36},... | collective-permute-start | bytes 98312 | tf_op jit(solution)/shard_map/ppermute | solution.py:375
  90.5 0.6 copy-start.9
  92.4 18.5 %all-to-all-start.3 = ((bf16[16,72,128]{2,1,0:T(8,128)(2,1)}), bf16[16,72,128]{2,1,0:T(8,128)(2,1)S(1)}, u32[]{:S(2)}, u32[]{:S(2)}) async-start(bf16[16,72,128]{2,1,0:T(8,128)(2,1)} %pair.1), calls=%async_computation.3 | async-start | bytes 589824 | tf_op jit(solution)/shard_map/all_to_all | solution.py:372
  96.9 1.6 %copy-start.3 = (bf16[8,2,512,128]{3,2,1,0:T(8,128)(2,1)S(1)}, bf16[8,2,512,128]{3,2,1,0:T(8,128)(2,1)}, u32[]{:S(2)}) copy-start(bf16[8,2,512,128]{3,2,1,0:T(8,128)(2,1)} %cv.5) | copy-start | bytes 6291460
  98.5 0.8 copy-start.10
  99.3 11.6 %copy-start.13 = (bf16[128]{0:T(256)(128)(2,1)S(1)}, bf16[128]{0:T(256)(128)(2,1)}, u32[]{:S(2)}) copy-start(bf16[128]{0:T(256)(128)(2,1)} %param.19) | copy-start | bytes 772
  99.3 39.4 %copy-start.4 = (bf16[4096,128]{1,0:T(8,128)(2,1)S(1)}, bf16[4096,128]{1,0:T(8,128)(2,1)}, u32[]{:S(2)}) copy-start(bf16[4096,128]{1,0:T(8,128)(2,1)} %w.3) | copy-start | bytes 3145732
  135.1 4.6 %collective-permute-start.4 = (bf16[16,32,128]{2,1,0:T(8,128)(2,1)S(1)}, bf16[16,32,128]{2,1,0:T(8,128)(2,1)S(1)}, u32[]{:S(2)}, u32[]{:S(2)}) collective-permute-start(bf16[16,32,128]{2,1,0:T(8,128)(2,1)S(1)} %all_to_all.27.src), channel_id=1, source_target_pairs={{0,4},{4,0},{8,12},{12,8},{16,20},{20,16},{24,28},{28,24},{32,36},... | collective-permute-start | bytes 393224 | tf_op jit(solution)/shard_map/ppermute | solution.py:375
  139.9 2.9 %collective-permute-start.5 = (bf16[128,128]{1,0:T(8,128)(2,1)S(1)}, bf16[128,128]{1,0:T(8,128)(2,1)S(1)}, u32[]{:S(2)}, u32[]{:S(2)}) collective-permute-start(bf16[128,128]{1,0:T(8,128)(2,1)S(1)} %shard_map.149.a), channel_id=1, source_target_pairs={{0,1},{1,0},{2,3},{3,2},{4,5},{5,4},{6,7},{7,6},{8,9},{9,8},{10,11... | collective-permute-start | bytes 98312 | tf_op jit(solution)/shard_map/ppermute | solution.py:557
  142.8 4.3 %collective-permute-start.6 = (bf16[128,128]{1,0:T(8,128)(2,1)S(1)}, bf16[128,128]{1,0:T(8,128)(2,1)S(1)}, u32[]{:S(2)}, u32[]{:S(2)}) collective-permute-start(bf16[128,128]{1,0:T(8,128)(2,1)S(1)} %shard_map.150.a), channel_id=1, source_target_pairs={{0,3},{1,2},{2,1},{3,0},{4,7},{5,6},{6,5},{7,4},{8,11},{9,10},{10,... | collective-permute-start | bytes 98312 | tf_op jit(solution)/shard_map/ppermute | solution.py:557

commit v4 on v2

--- a/solution.py
+++ b/solution.py
@@ -6,6 +6,7 @@
 from jax.experimental import pallas as pl
 from jax.experimental.pallas import tpu as pltpu
 from jax.sharding import PartitionSpec as P
+
 
 NEG_FILL = -1e30
 ROTARY_BASE = 10000.0
@@ -85,7 +86,7 @@
     @pl.when(pl.program_id(0) == 0)
     def _():
         r = linked[...]
-        for _step in range(5):
+        for _ in range(5):
             r = jnp.minimum(dot_nn(r, r), 1.0).astype(BF16)
         reach[...] = r
         depth[...] = dot_nt(jnp.ones((8, r.shape[1]), BF16), r) - 1.0
@@ -132,8 +133,9 @@
 
 
 def attend_kernel(
-    lengths, accepted, recv, reach, ck, cv, acc_out, stat_out, kf, vf, qs, *, qk, quarter, key_rows, side
+    lengths, accepted, recv, reach, ck, cv, acc_out, stat_out, fresh, qs, *, qk, quarter, key_rows, side
 ):
+    kf, vf = fresh.at[0], fresh.at[1]
     chips = recv.shape[0]
     group = qs.shape[0]
     parts = chips // (2 * group)
@@ -179,24 +181,23 @@
         seen = (reach[row0 : row0 + proposals].astype(F32) > 0.5) & (at >= 0) & (at < span)
         new = dot_nt(q, kf[...]).reshape(2 * group, proposals, n_tok)
         new = (new + jnp.where(seen, 0.0, NEG_FILL)[None]).reshape(n_rows, n_tok)
-        top = jnp.maximum(
-            jnp.max(old, axis=1, keepdims=True), jnp.max(new, axis=1, keepdims=True)
-        )
-        base = jnp.maximum(top, 0.5 * NEG_FILL)
-        w_old, w_new = jnp.exp(old - base), jnp.exp(new - base)
-        total = jnp.sum(w_old, axis=1, keepdims=True) + jnp.sum(w_new, axis=1, keepdims=True)
-        acc = dot_nn(w_old.astype(BF16), cv[b, g]) + dot_nn(w_new.astype(BF16), vf[...])
+        scores = jnp.concatenate([old, new], axis=1)
+        top = jnp.max(scores, axis=1, keepdims=True)
+        w = jnp.exp(scores - jnp.maximum(top, 0.5 * NEG_FILL))
+        total = jnp.sum(w, axis=1, keepdims=True)
+        w = w.astype(BF16)
+        acc = dot_nn(w[:, :span], cv[b, g]) + dot_nn(w[:, span:], vf[...])
         acc_out[b] = acc.astype(BF16)
         lanes = lax.broadcasted_iota(jnp.int32, (n_rows, 128), 1)
         stat = jnp.where(lanes == 0, top, jnp.where(lanes == 1, total, 0.0))
         stat_out[b] = stat.T[:8]
 
 
-def store_kernel(lengths, accepted, ck, cv, kn, vn, kfar, vfar, ko, vo):
+def store_kernel(lengths, accepted, ck, cv, fresh_near, fresh_far, ko, vo):
     me, _, core = place()
     b = pl.program_id(0)
     heads, span, width = ck.shape[1:]
-    n_tok = kn.shape[0]
+    n_tok = fresh_near.shape[1]
     proposals = n_tok // pl.num_programs(0)
     shift = me * span - lengths[b] - accepted[b]
     ko[...] = ck[...]
@@ -212,8 +213,8 @@
         written = (rel >= 0) & (rel < proposals)
         for g in range(heads):
             near = jnp.where(core == g, 1.0, 0.0)
-            for fresh_n, fresh_f, old, new in ((kn, kfar, ck, ko), (vn, vfar, cv, vo)):
-                fresh = fresh_n[...].astype(F32) * near + fresh_f[...].astype(F32) * (1.0 - near)
+            for n, (old, new) in enumerate(((ck, ko), (cv, vo))):
+                fresh = fresh_near[n].astype(F32) * near + fresh_far[n].astype(F32) * (1.0 - near)
                 placed = dot_nn(onehot, fresh.astype(BF16))
                 new[0, g] = jnp.where(written, placed, old[0, g].astype(F32)).astype(BF16)
 
@@ -417,12 +418,11 @@
                 attend_kernel, qk=qk, quarter=quarter, key_rows=key_rows, side=side
             ),
             in_specs=[SM, SM] + [VM] * 4,
-            out_specs=(VM,) * 4,
+            out_specs=(VM,) * 3,
             out_shape=(
                 sds((seqs, n_rows, v_dim), BF16),
                 sds((seqs, 8, n_rows), F32),
-                sds((n_tok, 2 * qk), BF16),
-                sds((n_tok, v_dim), BF16),
+                sds((2, n_tok, v_dim), BF16),
             ),
             scratch_shapes=[pltpu.VMEM((group, n_tok, 2 * qk), BF16)],
             compiler_params=limit(16),
@@ -434,9 +434,9 @@
             name="attend_far" if side else "attend_near",
         )(lengths, accepted, recv, reach, cache_keys, cache_values)
 
-    acc_near, stat_near, kn, vn = attend(0, near)
+    acc_near, stat_near, fresh_near = attend(0, near)
     acc_in, stat_in = swap(acc_near), swap(stat_near)
-    acc_far, stat_far, kfar, vfar = attend(1, far)
+    acc_far, stat_far, fresh_far = attend(1, far)
     half = group * proposals
     pieces = pl.pallas_call(
         pair_kernel,
@@ -448,11 +448,11 @@
     )(acc_far, stat_far, acc_in, stat_in)
     pieces = over_chips(pieces)
     cache_spec = pl.BlockSpec((1, local_kv, span, v_dim), lambda i: (i, 0, 0, 0))
-    fresh_spec = pl.BlockSpec((n_tok, v_dim), lambda i: (0, 0))
+    fresh_spec = pl.BlockSpec((2, n_tok, v_dim), lambda i: (0, 0, 0))
     keys_out, values_out = pl.pallas_call(
         store_kernel,
         grid=(seqs,),
-        in_specs=[SM, SM, cache_spec, cache_spec] + [fresh_spec] * 4,
+        in_specs=[SM, SM, cache_spec, cache_spec, fresh_spec, fresh_spec],
         out_specs=(cache_spec, cache_spec),
         out_shape=(sds(cache_keys.shape, BF16), sds(cache_values.shape, BF16)),
         compiler_params=limit(16),
@@ -462,7 +462,7 @@
             transcendentals=0,
         ),
         name="store",
-    )(lengths, accepted, cache_keys, cache_values, kn, vn, kfar, vfar)
+    )(lengths, accepted, cache_keys, cache_values, fresh_near, fresh_far)
     pieces, keys_out, values_out = lax.optimization_barrier((pieces, keys_out, values_out))
     first_head = (1 - core) * group + (chip % 2) * (group // 2)
     lam = lax.dynamic_slice_in_dim(mix_lambda, first_head, group // 2, 0)
@@ -482,7 +482,7 @@
     weight_spec = pl.BlockSpec((local_rows, out_cols), lambda i, tp: (tp[0], 0))
     term_spec = pl.BlockSpec((n_tok, out_cols), lambda i, tp: (0, 0))
 
-    def project_out(body, in_specs, dtype, name, *operands):
+    def project_out(body, in_specs, dtype, *operands):
         return pl.pallas_call(
             functools.partial(body, group=group),
             grid_spec=pltpu.PrefetchScalarGridSpec(
@@ -490,36 +490,33 @@
             ),
             out_shape=sds((n_tok, out_cols), dtype),
             compiler_params=limit(4),
-            name=name,
         )(lax.axis_index("tp").reshape(1), *operands)
 
     partial_term = project_out(
-        out_near_kernel, [heads_spec, weight_spec], F32, "out_near", heads_near, out_weight
+        out_near_kernel, [heads_spec, weight_spec], F32, heads_near, out_weight
     )
     term = project_out(
         out_far_kernel,
         [heads_spec, term_spec, weight_spec],
         BF16,
-        "out_far",
         heads_far,
         partial_term,
         out_weight,
     )
 
-    def add_from(x, hops, name):
+    def add_from(x, hops):
         return pl.pallas_call(
             add_kernel,
             out_shape=sds(x.shape, BF16),
             in_specs=[VM] * 2,
             out_specs=VM,
             compiler_params=limit(4),
-            name=name,
         )(x, lax.ppermute(x, "tp", hops))
 
     distance = 1
     while distance < tps:
         pairing = [(t, t // (2 * distance) * 2 * distance + 2 * distance - 1 - t % (2 * distance)) for t in range(tps)]
-        term = add_from(term, pairing, "sum_terms")
+        term = add_from(term, pairing)
         distance *= 2
     mixed = term
     return (mixed.reshape(seqs, proposals, out_cols), keys_out, values_out)

time: 146 us -> 146 us (level)
  no operation moved by 1% of the time
where the time goes in v4:
time: 146 us; the launch traced here: 144 us
  starting transfers between devices  49.7 us (34%)
  blocking collectives  41.5 us (28%)
  waiting for transfers between devices  24.2 us (17%)
  Pallas kernels  18 us (12%)
  local copies, waits for them, and re-layouts  7.98 us (5%)
  other arithmetic  1.57 us (1%)
    all_to_all x2, blocking collectives, over_chips(): lax.all_to_all(x, 'kv', 0, 0, axis_index_groups=same_core, tiled=True)  41.5 us
    all_to_all x2, starting transfers between devices, over_chips(): lax.all_to_all(x, 'kv', 0, 0, axis_index_groups=same_core, tiled=True)  30.6 us
    all_to_all x2, waiting for transfers between devices, over_chips(): lax.all_to_all(x, 'kv', 0, 0, axis_index_groups=same_core, tiled=True)  18.9 us
    ppermute x5, starting transfers between devices, swap(): return lax.ppermute(x, 'kv', pairs)  14.6 us
    pallas_call x2, Pallas kernels, attend(): pl.pallas_call(functools.partial(attend_kernel, qk=qk, quarter=quarter, k...  6.61 us
    unnamed x28, local copies, waits for them, and re-layouts  6.27 us
    ppermute x2, starting transfers between devices, add_from(): lax.ppermute(x, 'tp', hops)  4.48 us
    pallas_call x1, Pallas kernels, on_device(): pl.pallas_call(store_kernel, grid=(seqs,), in_specs=[SM, SM, cache_spec,...  4.04 us
  transfers between devices with their start and end apart: 9, of which 7 were waited for; matrix products, arithmetic and copies ran while one was open for 2% of the time, Pallas kernels for 6%

profile of v4, /device:TPU:33, one launch (start us, length us, event | category | flops | bytes accessed | tf_op | source)
XLA Modules:
  0.0 143.8 jit_solution(17779200607707623229)
XLA Ops:
  0.7 2.0 %prep.1 = bf16[16,96,128]{2,1,0:T(8,128)(2,1)} custom-call(bf16[128,1024]{1,0:T(8,128)(2,1)} %wq_hbm.1, bf16[128,256]{1,0:T(8,128)(2,1)} %wk_hbm.1, bf16[128,256]{1,0:T(8,128)(2,1)} %wv_hbm.1), custom_call_target="tpu_custom_call" | custom-call | tf_op jit(solution)/shard_map/prep/pallas_call | solution.py:343
  2.7 24.7 %all-to-all-start = ((bf16[16,96,128]{2,1,0:T(8,128)(2,1)}), bf16[16,96,128]{2,1,0:T(8,128)(2,1)S(1)}, u32[]{:S(2)}, u32[]{:S(2)}) async-start(bf16[16,96,128]{2,1,0:T(8,128)(2,1)} %prep.1), calls=%async_computation | async-start | bytes 786432 | tf_op jit(solution)/shard_map/all_to_all | solution.py:338
  29.8 1.2 copy-done.4
  31.0 1.5 %norm.1 = (bf16[128,4096]{1,0:T(8,128)(2,1)S(1)}, bf16[128,128]{1,0:T(8,128)(2,1)S(1)}, f32[8,128]{1,0:T(8,128)S(1)}) custom-call(bf16[128,4096]{1,0:T(8,128)(2,1)S(1)} %bitcast.6, bf16[1,4096]{1,0:T(2,128)(2,1)S(1)} %reshape.73.gain, bf16[128,128]{1,0:T(8,128)(2,1)S(1)} %fusion.2.linked), custom_call_target="tpu_custom_call" | custom-call | tf_op jit(solution)/shard_map/norm/pallas_call | solution.py:366
  33.8 11.4 %all-to-all-done.w = bf16[16,96,128]{2,1,0:T(8,128)(2,1)S(1)} async-done(((bf16[16,96,128]{2,1,0:T(8,128)(2,1)}), bf16[16,96,128]{2,1,0:T(8,128)(2,1)S(1)}, u32[]{:S(2)}, u32[]{:S(2)}) %all-to-all-start) | async-done | bytes 393248 | tf_op jit(solution)/shard_map/all_to_all | solution.py:338
  45.6 6.9 %collective-permute-start = (f32[48,128]{1,0:T(8,128)S(1)}, f32[48,128]{1,0:T(8,128)S(1)}, u32[]{:S(2)}, u32[]{:S(2)}) collective-permute-start(f32[48,128]{1,0:T(8,128)S(1)} %get-tuple-element.25), channel_id=1, source_target_pairs={{0,4},{4,0},{8,12},{12,8},{16,20},{20,16},{24,28},{28,24},{32,36},... | collective-permute-start | bytes 73736 | tf_op jit(solution)/shard_map/ppermute | solution.py:341
  52.5 0.8 collective-permute-done.recv
  54.2 18.3 %all_to_all.20.recv = bf16[16,48,128]{2,1,0:T(8,128)(2,1)S(1)} all-to-all(bf16[16,48,128]{2,1,0:T(8,128)(2,1)S(1)} %turn.1), channel_id=1, replica_groups={{0,8,16,24,32,40,48,56,64,72,80,88,96,104,112,120},{4,12,20,28,36,44,52..., dimensions={0} | all-to-all | bytes 393216 | tf_op jit(solution)/shard_map/all_to_all | solution.py:338
  73.3 3.3 %attend_near.1 = (bf16[8,128,128]{2,1,0:T(8,128)(2,1)S(1)}, f32[8,8,128]{2,1,0:T(8,128)S(1)}, bf16[2,128,128]{2,1,0:T(8,128)(2,1)S(1)}) custom-call(s32[8]{0:T(128)S(1)} %copy-done.10, s32[8]{0:T(128)S(1)} %copy-done.11, bf16[16,48,128]{2,1,0:T(8,128)(2,1)S(1)} %all_to_all.20.recv, bf16[128,128]{1,0:T(8,128)(2,1)S(1)} %copy-done.6, ...), custom_call_target="tpu_custom_call" | custom-call | flops 268435456 | bytes 2097152 | tf_op jit(solution)/shard_map/attend_near/pallas_call | solution.py:416
  76.6 3.5 %collective-permute-start.2 = (bf16[8,128,128]{2,1,0:T(8,128)(2,1)S(1)}, bf16[8,128,128]{2,1,0:T(8,128)(2,1)S(1)}, u32[]{:S(2)}, u32[]{:S(2)}) collective-permute-start(bf16[8,128,128]{2,1,0:T(8,128)(2,1)S(1)} %get-tuple-element.30), channel_id=1, source_target_pairs={{0,4},{4,0},{8,12},{12,8},{16,20},{20,16},{24,28},{28,24},{32,36},... | collective-permute-start | bytes 786440 | tf_op jit(solution)/shard_map/ppermute | solution.py:341
  80.6 0.9 collective-permute-done.1.recv
  81.5 3.3 %attend_far.1 = (bf16[8,128,128]{2,1,0:T(8,128)(2,1)S(1)}, f32[8,8,128]{2,1,0:T(8,128)S(1)}, bf16[2,128,128]{2,1,0:T(8,128)(2,1)S(1)}) custom-call(s32[8]{0:T(128)S(1)} %copy-done.10, s32[8]{0:T(128)S(1)} %copy-done.11, bf16[16,48,128]{2,1,0:T(8,128)(2,1)S(1)} %collective-permute-done.1.recv, bf16[128,128]{1,0:T(8,128)(2,1)S(1)} %copy-done.6, ...), custom_call_target="tpu_custom_call" | custom-call | flops 268435456 | bytes 2097152 | tf_op jit(solution)/shard_map/attend_far/pallas_call | solution.py:416
  85.5 1.3 pair.1
  86.8 6.0 %all-to-all-start.2 = ((bf16[16,72,128]{2,1,0:T(8,128)(2,1)}), bf16[16,72,128]{2,1,0:T(8,128)(2,1)S(1)}, u32[]{:S(2)}, u32[]{:S(2)}) async-start(bf16[16,72,128]{2,1,0:T(8,128)(2,1)} %pair.1), calls=%async_computation.2 | async-start | bytes 589824 | tf_op jit(solution)/shard_map/all_to_all | solution.py:338
  92.9 1.6 %copy-done.2 = bf16[8,2,512,128]{3,2,1,0:T(8,128)(2,1)S(1)} copy-done((bf16[8,2,512,128]{3,2,1,0:T(8,128)(2,1)S(1)}, bf16[8,2,512,128]{3,2,1,0:T(8,128)(2,1)}, u32[]{:S(2)}) %copy-start.2) | copy-done | bytes 2097176
  95.3 4.0 %store.1 = (bf16[8,2,512,128]{3,2,1,0:T(8,128)(2,1)}, bf16[8,2,512,128]{3,2,1,0:T(8,128)(2,1)}) custom-call(s32[8]{0:T(128)S(1)} %copy-done.10, s32[8]{0:T(128)S(1)} %copy-done.11, bf16[8,2,512,128]{3,2,1,0:T(8,128)(2,1)S(1)} %copy-done, bf16[8,2,512,128]{3,2,1,0:T(8,128)(2,1)S(1)} %copy-done.2, bf16[2,128,128]{2,1,0:T(8,128)(2,1)S(1)} %get-tuple-element.32.fresh_near, ...), custom_call_target="tpu_custom_call" | custom-call | flops 268435456 | bytes 8388608 | tf_op jit(solution)/shard_map/store/pallas_call | solution.py:452
  99.4 7.5 %all-to-all-done.2.recv = bf16[16,72,128]{2,1,0:T(8,128)(2,1)S(1)} async-done(((bf16[16,72,128]{2,1,0:T(8,128)(2,1)}), bf16[16,72,128]{2,1,0:T(8,128)(2,1)S(1)}, u32[]{:S(2)}, u32[]{:S(2)}) %all-to-all-start.2) | async-done | bytes 294944 | tf_op jit(solution)/shard_map/all_to_all | solution.py:338
  106.9 1.0 finish.1
  107.9 23.2 %all_to_all.21.src = bf16[16,32,128]{2,1,0:T(8,128)(2,1)S(1)} all-to-all(bf16[16,32,128]{2,1,0:T(8,128)(2,1)S(1)} %finish.1), channel_id=1, replica_groups={{0,8,16,24,32,40,48,56,64,72,80,88,96,104,112,120},{4,12,20,28,36,44,52..., dimensions={0} | all-to-all | bytes 262144 | tf_op jit(solution)/shard_map/all_to_all | solution.py:338
  131.1 3.6 %collective-permute-start.4 = (bf16[16,32,128]{2,1,0:T(8,128)(2,1)S(1)}, bf16[16,32,128]{2,1,0:T(8,128)(2,1)S(1)}, u32[]{:S(2)}, u32[]{:S(2)}) collective-permute-start(bf16[16,32,128]{2,1,0:T(8,128)(2,1)S(1)} %all_to_all.21.src), channel_id=1, source_target_pairs={{0,4},{4,0},{8,12},{12,8},{16,20},{20,16},{24,28},{28,24},{32,36},... | collective-permute-start | bytes 393224 | tf_op jit(solution)/shard_map/ppermute | solution.py:341
  135.9 1.5 %collective-permute-start.5 = (bf16[128,128]{1,0:T(8,128)(2,1)S(1)}, bf16[128,128]{1,0:T(8,128)(2,1)S(1)}, u32[]{:S(2)}, u32[]{:S(2)}) collective-permute-start(bf16[128,128]{1,0:T(8,128)(2,1)S(1)} %shard_map.149.a), channel_id=1, source_target_pairs={{0,1},{1,0},{2,3},{3,2},{4,5},{5,4},{6,7},{7,6},{8,9},{9,8},{10,11... | collective-permute-start | bytes 98312 | tf_op jit(solution)/shard_map/ppermute | solution.py:514
  137.4 1.4 collective-permute-done.5.b
  138.8 3.0 %collective-permute-start.6 = (bf16[128,128]{1,0:T(8,128)(2,1)S(1)}, bf16[128,128]{1,0:T(8,128)(2,1)S(1)}, u32[]{:S(2)}, u32[]{:S(2)}) collective-permute-start(bf16[128,128]{1,0:T(8,128)(2,1)S(1)} %shard_map.150.a), channel_id=1, source_target_pairs={{0,3},{1,2},{2,1},{3,0},{4,7},{5,6},{6,5},{7,4},{8,11},{9,10},{10,... | collective-permute-start | bytes 98312 | tf_op jit(solution)/shard_map/ppermute | solution.py:514
  141.8 1.3 collective-permute-done.6.b
  (50 shorter events, 9.6 us)
Async XLA Ops:
  0.6 71.9 %copy-start.10 = (s32[8]{0:T(128)S(1)}, s32[8]{0:T(128)}, u32[]{:S(2)}) copy-start(s32[8]{0:T(128)} %lengths.5) | copy-start | bytes 100
  0.6 71.9 %copy-start.11 = (s32[8]{0:T(128)S(1)}, s32[8]{0:T(128)}, u32[]{:S(2)}) copy-start(s32[8]{0:T(128)} %accepted.5) | copy-start | bytes 100
  2.6 69.9 %copy-start = (bf16[8,2,512,128]{3,2,1,0:T(8,128)(2,1)S(1)}, bf16[8,2,512,128]{3,2,1,0:T(8,128)(2,1)}, u32[]{:S(2)}) copy-start(bf16[8,2,512,128]{3,2,1,0:T(8,128)(2,1)} %ck.5) | copy-start | bytes 6291460
  2.7 42.5 %all-to-all-start = ((bf16[16,96,128]{2,1,0:T(8,128)(2,1)}), bf16[16,96,128]{2,1,0:T(8,128)(2,1)S(1)}, u32[]{:S(2)}, u32[]{:S(2)}) async-start(bf16[16,96,128]{2,1,0:T(8,128)(2,1)} %prep.1), calls=%async_computation | async-start | bytes 786432 | tf_op jit(solution)/shard_map/all_to_all | solution.py:338
  29.8 1.2 copy-start.4
  32.5 0.6 copy-start.5
  45.1 27.4 %copy-start.1 = (bf16[8,2,512,128]{3,2,1,0:T(8,128)(2,1)S(1)}, bf16[8,2,512,128]{3,2,1,0:T(8,128)(2,1)}, u32[]{:S(2)}) copy-start(bf16[8,2,512,128]{3,2,1,0:T(8,128)(2,1)} %cv.5) | copy-start | bytes 6291460
  45.6 7.8 %collective-permute-start = (f32[48,128]{1,0:T(8,128)S(1)}, f32[48,128]{1,0:T(8,128)S(1)}, u32[]{:S(2)}, u32[]{:S(2)}) collective-permute-start(f32[48,128]{1,0:T(8,128)S(1)} %get-tuple-element.25), channel_id=1, source_target_pairs={{0,4},{4,0},{8,12},{12,8},{16,20},{20,16},{24,28},{28,24},{32,36},... | collective-permute-start | bytes 73736 | tf_op jit(solution)/shard_map/ppermute | solution.py:341
  53.4 0.8 copy-start.7
  72.5 0.8 copy-start.6
  76.6 8.9 %collective-permute-start.2 = (bf16[8,128,128]{2,1,0:T(8,128)(2,1)S(1)}, bf16[8,128,128]{2,1,0:T(8,128)(2,1)S(1)}, u32[]{:S(2)}, u32[]{:S(2)}) collective-permute-start(bf16[8,128,128]{2,1,0:T(8,128)(2,1)S(1)} %get-tuple-element.30), channel_id=1, source_target_pairs={{0,4},{4,0},{8,12},{12,8},{16,20},{20,16},{24,28},{28,24},{32,36},... | collective-permute-start | bytes 786440 | tf_op jit(solution)/shard_map/ppermute | solution.py:341
  80.1 1.4 %collective-permute-start.1 = (bf16[16,48,128]{2,1,0:T(8,128)(2,1)S(1)}, bf16[16,48,128]{2,1,0:T(8,128)(2,1)S(1)}, u32[]{:S(2)}, u32[]{:S(2)}) collective-permute-start(bf16[16,48,128]{2,1,0:T(8,128)(2,1)S(1)} %all_to_all.20.recv), channel_id=1, source_target_pairs={{0,4},{4,0},{8,12},{12,8},{16,20},{20,16},{24,28},{28,24},{32,36},... | collective-permute-start | bytes 589832 | tf_op jit(solution)/shard_map/ppermute | solution.py:341
  80.2 12.6 %copy-start.13 = (f32[8]{0:T(128)S(1)}, f32[8]{0:T(128)}, u32[]{:S(2)}) copy-start(f32[8]{0:T(128)} %param.20) | copy-start | bytes 100
  80.2 5.3 %collective-permute-start.3 = (f32[8,8,128]{2,1,0:T(8,128)S(1)}, f32[8,8,128]{2,1,0:T(8,128)S(1)}, u32[]{:S(2)}, u32[]{:S(2)}) collective-permute-start(f32[8,8,128]{2,1,0:T(8,128)S(1)} %get-tuple-element.31), channel_id=1, source_target_pairs={{0,4},{4,0},{8,12},{12,8},{16,20},{20,16},{24,28},{28,24},{32,36},... | collective-permute-start | bytes 98312 | tf_op jit(solution)/shard_map/ppermute | solution.py:341
  84.8 0.6 copy-start.8
  86.8 20.1 %all-to-all-start.2 = ((bf16[16,72,128]{2,1,0:T(8,128)(2,1)}), bf16[16,72,128]{2,1,0:T(8,128)(2,1)S(1)}, u32[]{:S(2)}, u32[]{:S(2)}) async-start(bf16[16,72,128]{2,1,0:T(8,128)(2,1)} %pair.1), calls=%async_computation.2 | async-start | bytes 589824 | tf_op jit(solution)/shard_map/all_to_all | solution.py:338
  92.9 1.6 %copy-start.2 = (bf16[8,2,512,128]{3,2,1,0:T(8,128)(2,1)S(1)}, bf16[8,2,512,128]{3,2,1,0:T(8,128)(2,1)}, u32[]{:S(2)}) copy-start(bf16[8,2,512,128]{3,2,1,0:T(8,128)(2,1)} %cv.5) | copy-start | bytes 6291460
  94.5 0.8 copy-start.9
  95.3 11.6 %copy-start.12 = (bf16[128]{0:T(256)(128)(2,1)S(1)}, bf16[128]{0:T(256)(128)(2,1)}, u32[]{:S(2)}) copy-start(bf16[128]{0:T(256)(128)(2,1)} %param.19) | copy-start | bytes 772
  95.3 39.4 %copy-start.3 = (bf16[4096,128]{1,0:T(8,128)(2,1)S(1)}, bf16[4096,128]{1,0:T(8,128)(2,1)}, u32[]{:S(2)}) copy-start(bf16[4096,128]{1,0:T(8,128)(2,1)} %w.3) | copy-start | bytes 3145732
  131.1 4.6 %collective-permute-start.4 = (bf16[16,32,128]{2,1,0:T(8,128)(2,1)S(1)}, bf16[16,32,128]{2,1,0:T(8,128)(2,1)S(1)}, u32[]{:S(2)}, u32[]{:S(2)}) collective-permute-start(bf16[16,32,128]{2,1,0:T(8,128)(2,1)S(1)} %all_to_all.21.src), channel_id=1, source_target_pairs={{0,4},{4,0},{8,12},{12,8},{16,20},{20,16},{24,28},{28,24},{32,36},... | collective-permute-start | bytes 393224 | tf_op jit(solution)/shard_map/ppermute | solution.py:341
  135.9 2.9 %collective-permute-start.5 = (bf16[128,128]{1,0:T(8,128)(2,1)S(1)}, bf16[128,128]{1,0:T(8,128)(2,1)S(1)}, u32[]{:S(2)}, u32[]{:S(2)}) collective-permute-start(bf16[128,128]{1,0:T(8,128)(2,1)S(1)} %shard_map.149.a), channel_id=1, source_target_pairs={{0,1},{1,0},{2,3},{3,2},{4,5},{5,4},{6,7},{7,6},{8,9},{9,8},{10,11... | collective-permute-start | bytes 98312 | tf_op jit(solution)/shard_map/ppermute | solution.py:514
  138.8 4.3 %collective-permute-start.6 = (bf16[128,128]{1,0:T(8,128)(2,1)S(1)}, bf16[128,128]{1,0:T(8,128)(2,1)S(1)}, u32[]{:S(2)}, u32[]{:S(2)}) collective-permute-start(bf16[128,128]{1,0:T(8,128)(2,1)S(1)} %shard_map.150.a), channel_id=1, source_target_pairs={{0,3},{1,2},{2,1},{3,0},{4,7},{5,6},{6,5},{7,4},{8,11},{9,10},{10,... | collective-permute-start | bytes 98312 | tf_op jit(solution)/shard_map/ppermute | solution.py:514
